TPU v7x, 512 devices: a whole 4x4x16 slice. The times are simulated.
512 devices in a mesh: sp: 64 (over z, y), tp: 8 (over x, core).
Axes of the slice: x: 4, y: 4, z: 16, core: 2. Of those that a mesh axis runs over, the one named last changes fastest.
Arguments:
- hidden_in: bfloat16 [16384, 2048], P('sp'), may hold values from -16 to 16
- query_one: bfloat16 [2048, 512], P(None, 'tp'), may hold values from -0.13258252 to 0.13258252
- query_two: bfloat16 [2048, 512], P(None, 'tp'), may hold values from -0.13258252 to 0.13258252
- key_one: bfloat16 [2048, 512], P(None, 'tp'), may hold values from -0.13258252 to 0.13258252
- key_two: bfloat16 [2048, 512], P(None, 'tp'), may hold values from -0.13258252 to 0.13258252
- value_proj: bfloat16 [2048, 1024], P(None, 'tp'), may hold values from -0.125 to 0.125
- lambdas: float32 [8], P('tp'), may hold values from 0.3 to 0.8
- norm_gain: float32 [128], replicated, may hold values from 0.1 to 1.9
- out_proj: bfloat16 [1024, 2048], P('tp'), may hold values from -0.1875 to 0.1875
Outputs:
- attended: bfloat16 [16384, 2048], P('sp')
All inputs are finite; a program needn't handle non-finite values.
Results may differ from a plain program's by a relative error of at most 0.015.
Values may be sent and summed in bfloat16 or wider, within the bound.
A program may use at most 64 MiB of HBM per device.

v0:
```python
import math

import jax
import jax.numpy as jnp
from jax import lax
from jax.sharding import Mesh
from jax.sharding import PartitionSpec as P

SP = ("sp_0", "sp_1")


epsilon = 1e-06
masked_score = -1e30


def whole_of(x, axes, dim):
    if not axes:
        return x
    nearer = lax.all_gather(x, axes[-1], axis=dim, tiled=True)
    return whole_of(nearer, axes[:-1], dim)


def over_pieces(x, axis):
    parts = lax.all_gather(x, axis).astype(jnp.float32)
    return parts.sum(axis=0)


def shards(
    hidden_in, query_one, query_two, key_one, key_two, value_proj, lambdas, norm_gain, out_proj
):
    heads_dev = lambdas.shape[0]
    head_qk = query_one.shape[1] // heads_dev
    head_v = value_proj.shape[1] // heads_dev
    width_q = heads_dev * head_qk
    score_scale = 1.75 * head_qk ** (-0.5)
    joined = jnp.concatenate((query_one, query_two, key_one, key_two, value_proj), axis=1)
    projected = jnp.dot(hidden_in, joined, preferred_element_type=jnp.float32).astype(jnp.bfloat16)
    tok_rows = projected.shape[0]
    key_values = projected[:, 2 * width_q :]
    my_index = lax.axis_index(SP)
    offset = my_index * tok_rows
    query_sets = (projected[:, : 2 * width_q],)
    position_sets = (offset + jnp.arange(tok_rows, dtype=jnp.int32),)
    groups = []
    for query_rows, positions in zip(query_sets, position_sets):
        group_rows = query_rows.shape[0]
        query_a = query_rows[:, :width_q].reshape(group_rows, heads_dev, head_qk)
        query_b = query_rows[:, width_q:].reshape(group_rows, heads_dev, head_qk)
        groups.append((query_a, query_b, positions, positions[group_rows - 1]))

    def one_map(queries, keys, value_rows, allowed, running_max, running_sum, accum):
        scores = (
            jnp.einsum("qhd,khd->hqk", queries, keys, preferred_element_type=jnp.float32)
            * score_scale
        )
        scores = jnp.where(allowed[None], scores, masked_score)
        new_max = jnp.maximum(running_max, jnp.max(scores, axis=-1))
        rescale = jnp.exp(running_max - new_max)
        weights = jnp.where(allowed[None], jnp.exp(scores - new_max[..., None]), 0.0)
        new_sum = running_sum * rescale + jnp.sum(weights, axis=-1)
        added = jnp.einsum(
            "hqk,khe->hqe",
            weights.astype(jnp.bfloat16),
            value_rows,
            preferred_element_type=jnp.float32,
        )
        return (new_max, new_sum, accum * rescale[..., None] + added)

    def absorb(group_state, group, kblock, kstart):
        query_a, query_b, positions, last_pos = group
        block_rows = kblock.shape[0]
        k_pos = kstart + jnp.arange(block_rows, dtype=jnp.int32)
        allowed = k_pos[None, :] <= positions[:, None]
        keys_a = kblock[:, :width_q].reshape(block_rows, heads_dev, head_qk)
        keys_b = kblock[:, width_q : 2 * width_q].reshape(block_rows, heads_dev, head_qk)
        value_rows = kblock[:, 2 * width_q :].reshape(block_rows, heads_dev, head_v)
        first_map = one_map(query_a, keys_a, value_rows, allowed, *group_state[:3])
        second_map = one_map(query_b, keys_b, value_rows, allowed, *group_state[3:])
        return first_map + second_map

    group = groups[0]
    group_rows = group[0].shape[0]
    start_max = jnp.full((heads_dev, group_rows), masked_score, jnp.float32)
    start_sum = jnp.zeros((heads_dev, group_rows), jnp.float32)
    start_acc = jnp.zeros((heads_dev, group_rows, head_v), jnp.float32)
    initial_list = [(start_max, start_sum, start_acc, start_max, start_sum, start_acc)]
    initial = tuple(initial_list)
    softmax_state = initial
    kv_piece = whole_of(key_values, SP, 0)
    piece_rows = kv_piece.shape[0]
    block_rows = math.gcd(piece_rows, 512)
    block_count = piece_rows // block_rows
    stacked = kv_piece.reshape(block_count, block_rows, kv_piece.shape[1])

    def absorb_step(carried, blocks_in):
        kblock, block_index = blocks_in
        kstart = block_index * block_rows
        renewed = []
        for group, group_state in zip(groups, carried):
            renewed.append(
                lax.cond(
                    kstart <= group[3],
                    lambda inner, group=group: absorb(inner, group, kblock, kstart),
                    lambda inner: inner,
                    group_state,
                )
            )
        return (tuple(renewed), None)

    softmax_state, _ = lax.scan(
        absorb_step, softmax_state, (stacked, jnp.arange(block_count, dtype=jnp.int32))
    )
    normed_sets = []
    for group_state in softmax_state:
        out_a = group_state[2] / group_state[1][..., None]
        out_b = group_state[5] / group_state[4][..., None]
        mixed_out = out_a - lambdas[:, None, None] * out_b
        scale_rows = lax.rsqrt(jnp.mean(mixed_out * mixed_out, axis=-1, keepdims=True) + epsilon)
        normed = (mixed_out * scale_rows * norm_gain).astype(jnp.bfloat16)
        group_rows = normed.shape[1]
        normed_sets.append(jnp.transpose(normed, (1, 0, 2)).reshape(group_rows, heads_dev * head_v))
    normed_all = normed_sets[0]
    partial_value = jnp.dot(normed_all, out_proj, preferred_element_type=jnp.float32)
    result = over_pieces(partial_value.astype(jnp.bfloat16), "tp").astype(jnp.float32)
    return result.astype(jnp.bfloat16)


def solution(mesh):
    torus = Mesh(mesh.devices.reshape(16, 4, mesh.shape["tp"]), ("sp_0", "sp_1", "tp"))
    placed = (
        P(SP, None),
        P(None, "tp"),
        P(None, "tp"),
        P(None, "tp"),
        P(None, "tp"),
        P(None, "tp"),
        P("tp"),
        P(),
        P("tp", None),
    )
    return jax.shard_map(
        shards, mesh=torus, in_specs=placed, out_specs=P(SP, None), check_vma=False
    )
```

profile of v0, /device:TPU:1, one launch (start us, length us, event | category | flops | bytes accessed | tf_op | source)
XLA Modules:
  0.0 361.6 jit_solution(14806410718348674276)
XLA Ops:
  6.5 1.3 copy.17
  7.9 1.2 copy.18
  9.1 1.2 copy.19
  10.6 3.8 %concatenate.3 = bf16[2048,384]{1,0:T(8,128)(2,1)} concatenate(bf16[2048,64]{1,0:T(8,128)(2,1)S(1)} %copy.17, bf16[2048,64]{1,0:T(8,128)(2,1)S(1)} %copy.18, bf16[2048,64]{1,0:T(8,128)(2,1)S(1)} %copy.19, bf16[2048,64]{1,0:T(8,128)(2,1)S(1)} %copy.20, bf16[2048,128]{1,0:T(8,128)(2,1)} %param.18), dimensions={1} | concatenate | bytes 3145728 | tf_op jit(solution)/shard_map/concatenate | solution.py:36
  14.5 2.0 fusion.30
  16.5 12.6 %all_gather.12 = bf16[1024,256]{0,1:T(8,128)(2,1)} all-gather(bf16[256,256]{0,1:T(8,128)(2,1)S(1)} %slice.34), channel_id=1, replica_groups=mesh['sp_0'=16,'sp_1'=4,'tp'=8] {'sp_1'}, dimensions={0}, use_global_device_ids=true | all-gather | bytes 655360 | tf_op jit(solution)/shard_map/all_gather | solution.py:19
  29.2 0.6 slice.27
  30.4 111.2 %all-gather.4.cloned.1.call-done = bf16[16384,256]{0,1:T(8,128)(2,1)} async-done(((bf16[1024,256]{0,1:T(8,128)(2,1)}), bf16[16384,256]{0,1:T(8,128)(2,1)}) %all-gather.4.cloned.1.call-update) | async-done | bytes 8388624 | tf_op jit(solution)/shard_map/all_gather | solution.py:19
  141.7 11.9 %copy.22 = bf16[16384,256]{1,0:T(8,128)(2,1)} copy(bf16[16384,256]{0,1:T(8,128)(2,1)} %all-gather.4.cloned.1.call-done) | data formatting | bytes 16777216
  153.7 59.1 %while.21 = (s32[]{:T(128)}, f32[1,256]{1,0:T(1,128)S(1)}, f32[1,256]{1,0:T(1,128)S(1)}, f32[1,256,128]{2,1,0:T(8,128)S(1)}, f32[1,256]{1,0:T(1,128)S(1)}, /*ind...) while((s32[]{:T(128)}, f32[1,256]{1,0:T(1,128)S(1)}, ...), condition=%wide.region_7.8_spmd.clone, body=%wide.region_0.7_spmd.clone.sunk | while | flops 103810816 | bytes 4837775 | solution.py:110
  153.8 0.6 dynamic_slice.13
  155.5 2.7 conditional.3
  155.5 1.0 dynamic-slice_bitcast_fusion
  158.2 0.6 dynamic_slice.13
  160.0 0.6 dynamic_slice.13
  161.8 0.6 dynamic_slice.13
  163.5 0.6 dynamic_slice.13
  165.3 0.6 dynamic_slice.13
  167.0 0.6 dynamic_slice.13
  168.8 0.6 dynamic_slice.13
  170.6 0.6 dynamic_slice.13
  172.3 0.6 dynamic_slice.13
  174.1 0.6 dynamic_slice.13
  175.8 0.6 dynamic_slice.13
  177.6 0.6 dynamic_slice.13
  198.7 0.6 dynamic_slice.13
  200.5 0.6 dynamic_slice.13
  202.3 0.6 dynamic_slice.13
  204.0 0.6 dynamic_slice.13
  213.1 1.4 convolution_convert_fusion
  214.6 133.8 %all-gather.6.cloned.1.call-done = bf16[2048,2048]{1,0:T(8,128)(2,1)} async-done(((bf16[256,2048]{1,0:T(8,128)(2,1)}), bf16[2048,2048]{1,0:T(8,128)(2,1)}) %all-gather.6.cloned.1.call-update) | async-done | bytes 8388624 | tf_op jit(solution)/shard_map/all_gather | solution.py:24
  348.4 6.4 %reduce_sum.44 = bf16[256,2048]{1,0:T(8,128)(2,1)} reduce(bf16[8,256,2048]{2,1,0:T(8,128)(2,1)} %bitcast.59, bf16[]{:T(256)} %constant.53.clone.1), dimensions={0}, to_apply=%region_9.10 | reduce | flops 3670016 | bytes 9437186 | tf_op jit(solution)/shard_map/reduce_sum | solution.py:25
  (115 shorter events, 11.2 us)
Async XLA Ops:
  6.5 7.9 %copy-start = (bf16[256,2048]{1,0:T(8,128)(2,1)S(1)}, bf16[256,2048]{1,0:T(8,128)(2,1)}, u32[]{:S(2)}) copy-start(bf16[256,2048]{1,0:T(8,128)(2,1)} %param.13) | copy-start | bytes 3145732
  6.5 3.8 %copy-start.2 = (bf16[2048,64]{0,1:T(8,128)(2,1)S(1)}, bf16[2048,64]{0,1:T(8,128)(2,1)}, u32[]{:S(2)}) copy-start(bf16[2048,64]{0,1:T(8,128)(2,1)} %param.17) | copy-start | bytes 786436
  6.5 135.2 %all-gather.4.cloned.1.call-start = ((), (), s32[]{:S(2)}) async-start(), calls=%async_computation | async-start | bytes 8912896 | tf_op jit(solution)/shard_map/all_gather | solution.py:19
  29.1 319.3 %all-gather.6.cloned.1.call-start = ((), (), s32[]{:S(2)}) async-start(), calls=%async_computation.1 | async-start | bytes 9437184 | tf_op jit(solution)/shard_map/all_gather | solution.py:24
  153.7 59.4 %copy-start.1 = (bf16[128,2048]{1,0:T(8,128)(2,1)S(1)}, bf16[128,2048]{1,0:T(8,128)(2,1)}, u32[]{:S(2)}) copy-start(bf16[128,2048]{1,0:T(8,128)(2,1)} %param.21) | copy-start | bytes 1572868
  153.7 59.3 %copy-start.3 = (f32[128]{0:T(128)S(1)}, f32[128]{0:T(128)}, u32[]{:S(2)}) copy-start(f32[128]{0:T(128)} %param.20) | copy-start | bytes 1540
Sparse Core Ops, SparseCore 0:
  29.2 112.4 all-gather.3
  214.7 133.6 all-gather.5
where the time goes:
time: 364 us; the launch traced here: 362 us
  waiting for transfers between devices  245 us (67%)
  local copies, waits for them, and re-layouts  39.3 us (11%)
  loops' own time  38.6 us (11%)
  between operations  14.2 us (4%)
  blocking collectives  12.6 us (3%)
  other arithmetic  6.89 us (2%)
  matrix products  4.87 us (1%)
    all_gather x1, waiting for transfers between devices, over_pieces(): parts = lax.all_gather(x, axis).astype(jnp.float32)  134 us
    all_gather x1, waiting for transfers between devices, whole_of(): nearer = lax.all_gather(x, axes[-1], axis=dim, tiled=True)  111 us
    another operation x1, loops' own time, shards(): lax.scan(absorb_step, softmax_state, (stacked, jnp.arange(block_count, dt...  38.1 us
    dynamic_slice x32, local copies, waits for them, and re-layouts, shards(): lax.scan(absorb_step, softmax_state, (stacked, jnp.arange(block_count, dt...  17.7 us
    unnamed x13, local copies, waits for them, and re-layouts  16 us
    all_gather x1, blocking collectives, whole_of(): nearer = lax.all_gather(x, axes[-1], axis=dim, tiled=True)  12.6 us
  transfers between devices with their start and end apart: 2, of which 2 were waited for; matrix products, arithmetic and copies ran while one was open for 0% of the time, Pallas kernels for 0%

commit v1 on v0

v1 whole, which is shorter than its diff:
```python
import math

import jax
import jax.numpy as jnp
from jax import lax
from jax.experimental import pallas as pl
from jax.experimental.pallas import tpu as pltpu
from jax.sharding import Mesh
from jax.sharding import PartitionSpec as P

SP = ("sp_0", "sp_1")
F32 = jnp.float32
BF16 = jnp.bfloat16
MESH = pl.DeviceIdType.MESH

epsilon = 1e-06
masked_score = -1e30

NZ = 16
NY = 4
NX = 4
HALF = NZ // 2
CHUNKS = 4
FAR = 2


def kernel(
    hidden_hbm, wq1_hbm, wq2_hbm, wk1_hbm, wk2_hbm, wv_hbm, lam_ref, gain_ref, wo_hbm,
    out_hbm,
    hid, wq, wk, wv, load_sem,
    kv, kv_send, kv_recv,
    qbuf, qz, q_send, q_recv,
    m_ref, l_ref, acc_ref,
    opart, stats, orecv, strecv, relay, o_send, o_recv, rel_send, rel_recv, st_send, st_recv,
    wo, wo_send, wo_recv, wo_dsend, wo_drecv,
    nb, nb_send, nb_recv, nb_dsend, nb_drecv,
    out_v, out_sem,
):
    z = lax.axis_index("sp_0")
    y = lax.axis_index("sp_1")
    t = lax.axis_index("tp")
    x = t // 2
    core = t % 2
    rows = hid.shape[0]
    head_qk = wq.shape[1]
    head_v = wv.shape[1]
    half_rows = rows // 2
    scale = 1.75 * head_qk ** (-0.5) * math.log2(math.e)

    z_up, z_down = (z + 1) % NZ, (z + NZ - 1) % NZ
    y_at = [y, (y + 1) % NY, (y + 2) % NY, (y + 3) % NY]
    x_at = [x, (x + 1) % NX, (x + 2) % NX, (x + 3) % NX]
    tp_at = [2 * xx + core for xx in x_at]
    sibling = 2 * x + (1 - core)

    loads = [
        pltpu.make_async_copy(hidden_hbm, hid, load_sem.at[0]),
        pltpu.make_async_copy(wk1_hbm, wk.at[0], load_sem.at[1]),
        pltpu.make_async_copy(wk2_hbm, wk.at[1], load_sem.at[2]),
        pltpu.make_async_copy(wv_hbm, wv, load_sem.at[3]),
        pltpu.make_async_copy(wq1_hbm, wq.at[0], load_sem.at[4]),
        pltpu.make_async_copy(wq2_hbm, wq.at[1], load_sem.at[5]),
        pltpu.make_async_copy(wo_hbm, wo.at[t], load_sem.at[6]),
    ]
    for load in loads:
        load.start()

    barrier = pltpu.get_barrier_semaphore()
    partners = [
        {"sp_0": z_up}, {"sp_0": z_down},
        {"sp_1": y_at[1]}, {"sp_1": y_at[2]}, {"sp_1": y_at[3]},
        {"tp": tp_at[1]}, {"tp": tp_at[3]}, {"tp": sibling},
    ]
    for partner in partners:
        pl.semaphore_signal(barrier, inc=1, device_id=partner, device_id_type=MESH)

    def remote(src, dst, send_sem, recv_sem, device):
        return pltpu.make_async_remote_copy(
            src_ref=src, dst_ref=dst, send_sem=send_sem, recv_sem=recv_sem,
            device_id=device, device_id_type=MESH,
        )

    def project(h, pair):
        both = pair[...].reshape(2 * head_qk, pair.shape[2])
        return lax.dot_general(h, both, (((1,), (1,)), ((), ())), preferred_element_type=F32)

    for load in loads[:4]:
        load.wait()
    h = hid[...]
    k = project(h, wk)
    v = jnp.dot(h, wv[...], preferred_element_type=F32)
    own = jnp.concatenate((k, v), axis=1).astype(BF16)
    kv[z] = own.reshape(kv.shape[1:])

    pl.semaphore_wait(barrier, len(partners))

    def up(step, chunk, slot):
        ref = kv.at[slot, chunk]
        return remote(
            ref, ref, kv_send.at[0, step - 1, chunk], kv_recv.at[0, step - 1, chunk], {"sp_0": z_up}
        )

    def down(step, chunk, slot):
        ref = kv.at[slot, chunk]
        return remote(
            ref, ref, kv_send.at[1, step - 1, chunk], kv_recv.at[1, step - 1, chunk], {"sp_0": z_down}
        )

    for chunk in range(CHUNKS):
        up(1, chunk, z).start()
        down(1, chunk, z).start()

    loads[4].wait()
    loads[5].wait()
    qbuf[y] = project(h, wq).astype(BF16)

    def q_copy(off, slot):
        return remote(
            qbuf.at[slot], qbuf.at[slot], q_send.at[off], q_recv.at[off], {"sp_1": y_at[off]}
        )

    for off in (2, 1, 3):
        q_copy(off, y).start()

    def gather_ops(buf, send, recv, dsend, drecv):
        first = {0: 0, 1: 1}

        def hop(direction, order, slot):
            piece = first[direction] if order != 1 else 1 - first[direction]
            ref = buf.at[slot, piece]
            to = tp_at[1] if direction == 0 else tp_at[3]
            return remote(ref, ref, send.at[direction, order], recv.at[direction, order], {"tp": to})

        def across(index, piece, slot):
            ref = buf.at[slot, piece]
            return remote(ref, ref, dsend.at[index, piece], drecv.at[index, piece], {"tp": sibling})

        def start_own():
            for order in range(2):
                for direction in range(2):
                    hop(direction, order, t).start()
            for piece in range(2):
                across(0, piece, t).start()

        def came(direction):
            return tp_at[3] if direction == 0 else tp_at[1]

        def take(order):
            for direction in range(2):
                slot = tp_at[2] if order == 2 else came(direction)
                arrived = hop(direction, order, slot)
                arrived.wait_recv()
                piece = first[direction] if order != 1 else 1 - first[direction]
                if order == 0:
                    hop(direction, 2, slot).start()
                index = 2 if order == 2 else (3 if direction == 0 else 1)
                across(index, piece, slot).start()

        def take_across():
            for index in range(4):
                slot = 2 * x_at[index] + (1 - core)
                for piece in range(2):
                    across(index, piece, slot).wait_recv()

        def drain():
            for direction in range(2):
                for order in range(3):
                    slot = came(direction) if order == 2 else t
                    hop(direction, order, slot).wait_send()
            for index in range(4):
                for piece in range(2):
                    across(index, piece, tp_at[index]).wait_send()

        return start_own, take, take_across, drain

    wo_start, wo_take, wo_take_across, wo_drain = gather_ops(wo, wo_send, wo_recv, wo_dsend, wo_drecv)
    nb_start, nb_take, nb_take_across, nb_drain = gather_ops(nb, nb_send, nb_recv, nb_dsend, nb_drecv)

    loads[6].wait()
    wo_start()

    for off in (1, 3, 2):
        q_copy(off, y_at[(NY - off) % NY]).wait_recv()
    lane = lax.broadcasted_iota(jnp.int32, (rows, 2 * head_qk), 1)
    in_first = (lane < head_qk).astype(F32)

    def split_queries(block, _):
        q = qbuf[block].astype(F32)
        qz[0, block] = (q * in_first).astype(BF16)
        qz[1, block] = (q * (1.0 - in_first)).astype(BF16)
        return 0

    lax.fori_loop(0, NY, split_queries, 0)

    def block_of(slot):
        whole = kv[slot].reshape(rows, 2 * head_qk + head_v)
        return whole[:, : 2 * head_qk], whole[:, 2 * head_qk :]

    def attend(block, keys, vals, allowed=None):
        for pick in range(2):
            scores = scale * lax.dot_general(
                qz[pick, block], keys, (((1,), (1,)), ((), ())), preferred_element_type=F32
            )
            if allowed is not None:
                scores = jnp.where(allowed, scores, masked_score)
            highest = jnp.max(scores, axis=1, keepdims=True)
            if allowed is None:
                before = m_ref[pick, block]
                now = jnp.maximum(before, highest)
                rescale = jnp.exp2(before - now)
            else:
                now = jnp.broadcast_to(highest, (rows, 128))
            parts = []
            total = None
            for left in range(0, scores.shape[1], 128):
                part = jnp.exp2(scores[:, left : left + 128] - now)
                if allowed is not None:
                    part = jnp.where(allowed[:, left : left + 128], part, 0.0)
                total = part if total is None else total + part
                parts.append(part.astype(BF16))
            added = jnp.dot(jnp.concatenate(parts, axis=1), vals, preferred_element_type=F32)
            m_ref[pick, block] = now
            if allowed is None:
                l_ref[pick, block] = l_ref[pick, block] * rescale + total
                acc_ref[pick, block] = acc_ref[pick, block] * rescale + added
            else:
                l_ref[pick, block] = total
                acc_ref[pick, block] = added

    def pass_on(step, chunk):
        low, high = (z + NZ - step) % NZ, (z + step) % NZ
        up(step, chunk, low).wait_recv()

        @pl.when((step < HALF - 1) | (chunk < CHUNKS // 2))
        def _():
            up(step + 1, chunk, low).start()

        down(step, chunk, high).wait_recv()

        @pl.when((step < HALF - 1) | (chunk >= CHUNKS // 2))
        def _():
            down(step + 1, chunk, high).start()

    def attend_pair(step, block):
        low, high = (z + NZ - step) % NZ, (z + step) % NZ

        @pl.when(z >= NZ - step)
        def _():
            keys_low, vals_low = block_of(low)
            keys_high, vals_high = block_of(high)
            attend(
                block,
                jnp.concatenate((keys_low, keys_high), axis=0),
                jnp.concatenate((vals_low, vals_high), axis=0),
            )

        @pl.when((z >= step) & (z < NZ - step))
        def _():
            attend(block, *block_of(low))

    def first_step(block, _):
        pass_on(1, block)
        q_pos = block * rows + lax.broadcasted_iota(jnp.int32, (rows, rows), 0)
        k_pos = y * rows + lax.broadcasted_iota(jnp.int32, (rows, rows), 1)
        attend(block, *block_of(z), allowed=k_pos <= q_pos)
        return 0

    lax.fori_loop(0, NY, first_step, 0)

    def ring_step(index, _):
        step, block = index // CHUNKS, index % CHUNKS
        pass_on(step, block)

        @pl.when(index == 4 * CHUNKS)
        def _():
            wo_take(0)

        @pl.when(index == 6 * CHUNKS)
        def _():
            wo_take(1)

        attend_pair(step - 1, block)
        return 0

    lax.fori_loop(2 * CHUNKS, HALF * CHUNKS, ring_step, 0)

    def last_pair(block, _):
        attend_pair(HALF - 1, block)
        return 0

    lax.fori_loop(0, NY, last_pair, 0)

    opposite = (z + HALF) % NZ
    for chunk in range(CHUNKS):
        if chunk < CHUNKS // 2:
            up(HALF, chunk, opposite).wait_recv()
        else:
            down(HALF, chunk, opposite).wait_recv()

    def o_copy(direction, piece, slot):
        to = y_at[1] if direction == 0 else y_at[3]
        return remote(
            opart.at[slot, piece], orecv.at[direction, piece],
            o_send.at[direction, piece], o_recv.at[direction, piece], {"sp_1": to},
        )

    def rel_copy(direction, slot):
        to = y_at[1] if direction == 0 else y_at[3]
        return remote(
            opart.at[slot, direction], relay.at[direction],
            rel_send.at[direction, 0], rel_recv.at[direction, 0], {"sp_1": to},
        )

    def rel_forward(direction):
        to = y_at[1] if direction == 0 else y_at[3]
        return remote(
            relay.at[direction], orecv.at[2, direction],
            rel_send.at[direction, 1], rel_recv.at[direction, 1], {"sp_1": to},
        )

    def st_copy(off, slot):
        return remote(
            stats.at[slot], strecv.at[off], st_send.at[off], st_recv.at[off], {"sp_1": y_at[off]}
        )

    lane_128 = lax.broadcasted_iota(jnp.int32, (rows, 128), 1)

    def finish(block):
        @pl.when(z >= HALF)
        def _():
            attend(block, *block_of(opposite))

        table = jnp.zeros((rows, 128), F32)
        for pick in range(2):
            total = jnp.sum(l_ref[pick, block], axis=1, keepdims=True)
            table = jnp.where(lane_128 == 2 * pick, m_ref[pick, block], table)
            table = jnp.where(lane_128 == 2 * pick + 1, total, table)
        stats[block] = table.T[:8]
        packed = jnp.concatenate((acc_ref[0, block], acc_ref[1, block]), axis=1).astype(BF16)
        opart[block] = packed.reshape(opart.shape[1:])

    finish(y_at[2])
    rel_copy(0, y_at[2]).start()
    rel_copy(1, y_at[2]).start()
    st_copy(2, y_at[2]).start()
    finish(y_at[1])
    o_copy(0, 0, y_at[1]).start()
    o_copy(0, 1, y_at[1]).start()
    st_copy(1, y_at[1]).start()
    finish(y_at[3])
    o_copy(1, 0, y_at[3]).start()
    o_copy(1, 1, y_at[3]).start()
    st_copy(3, y_at[3]).start()
    finish(y_at[0])

    wo_take(2)

    for direction in range(2):
        rel_copy(direction, y_at[2]).wait_recv()
        rel_forward(direction).start()

    for off in range(1, NY):
        st_copy(off, y_at[0]).wait_recv()

    lam = lam_ref[0]
    tables = [stats[y], strecv[1], strecv[3], strecv[2]]
    coefs = []
    for pick in range(2):
        maxima = [table[2 * pick : 2 * pick + 1] for table in tables]
        sums = [table[2 * pick + 1 : 2 * pick + 2] for table in tables]
        highest = maxima[0]
        for other in maxima[1:]:
            highest = jnp.maximum(highest, other)
        shares = [jnp.exp2(one - highest) for one in maxima]
        total = shares[0] * sums[0]
        for share, one in zip(shares[1:], sums[1:]):
            total = total + share * one
        factor = (1.0 if pick == 0 else -lam) / total
        coefs.extend(share * factor for share in shares)
    coef_rows = jnp.concatenate(coefs, axis=0)
    coef_cols = jnp.concatenate([coef_rows] * 16, axis=0).T

    gain = gain_ref[...].reshape(1, head_v)
    for piece in range(2):
        o_copy(0, piece, y_at[1]).wait_recv()
        o_copy(1, piece, y_at[3]).wait_recv()
        rel_forward(piece).wait_recv()
        part = slice(piece * half_rows, (piece + 1) * half_rows)
        cols = coef_cols[part]
        arrived = [None] + [orecv[source, piece].astype(F32) for source in (0, 1, 2)]
        mixed = acc_ref[0, y, part] * cols[:, 0:1] + acc_ref[1, y, part] * cols[:, 4:5]
        for source in (1, 2, 3):
            mixed = mixed + arrived[source][:, :head_v] * cols[:, source : source + 1]
            mixed = mixed + arrived[source][:, head_v:] * cols[:, 4 + source : 5 + source]
        spread = lax.rsqrt(jnp.mean(mixed * mixed, axis=1, keepdims=True) + epsilon)
        nb[t, piece] = (mixed * spread * gain).astype(BF16)

    nb_start()
    wo_take_across()
    nb_take(0)
    nb_take(1)
    nb_take(2)
    nb_take_across()

    lhs = jnp.concatenate([nb[head].reshape(rows, head_v) for head in range(2 * NX)], axis=1)
    width = 256
    out_copies = []
    for left in range(0, out_v.shape[1], width):
        rhs = wo[:, :, :, left : left + width].reshape(2 * NX * head_v, width)
        out_v[:, left : left + width] = jnp.dot(lhs, rhs, preferred_element_type=F32).astype(BF16)
        copy = pltpu.make_async_copy(
            out_v.at[:, left : left + width], out_hbm.at[:, left : left + width],
            out_sem.at[left // width],
        )
        copy.start()
        out_copies.append(copy)

    def drain_ring(index, _):
        step, chunk = index // CHUNKS, index % CHUNKS

        @pl.when((step < HALF) | (chunk < CHUNKS // 2))
        def _():
            up(step, chunk, z).wait_send()

        @pl.when((step < HALF) | (chunk >= CHUNKS // 2))
        def _():
            down(step, chunk, z).wait_send()

        return 0

    lax.fori_loop(CHUNKS, (HALF + 1) * CHUNKS, drain_ring, 0)
    for off in range(1, NY):
        q_copy(off, y).wait_send()
        st_copy(off, y).wait_send()
    for direction in range(2):
        for piece in range(2):
            o_copy(direction, piece, y).wait_send()
        rel_copy(direction, y).wait_send()
        rel_forward(direction).wait_send()
    wo_drain()
    nb_drain()
    for copy in out_copies:
        copy.wait()


def shards(
    hidden_in, query_one, query_two, key_one, key_two, value_proj, lambdas, norm_gain, out_proj
):
    rows, depth = hidden_in.shape
    head_qk = query_one.shape[1]
    head_v = value_proj.shape[1]
    wide = 2 * head_qk + head_v
    half = rows // 2
    heads = 2 * NX
    dma = pltpu.SemaphoreType.DMA
    anywhere = pl.BlockSpec(memory_space=pl.ANY)
    scratch = [
        pltpu.VMEM((rows, depth), BF16),
        pltpu.VMEM((2, head_qk, depth), BF16),
        pltpu.VMEM((2, head_qk, depth), BF16),
        pltpu.VMEM((depth, head_v), BF16),
        dma((7,)),
        pltpu.VMEM((NZ, CHUNKS, rows // CHUNKS, wide), BF16),
        dma((2, HALF, CHUNKS)),
        dma((2, HALF, CHUNKS)),
        pltpu.VMEM((NY, rows, 2 * head_qk), BF16),
        pltpu.VMEM((2, NY, rows, 2 * head_qk), BF16),
        dma((NY,)),
        dma((NY,)),
        pltpu.VMEM((2, NY, rows, 128), F32),
        pltpu.VMEM((2, NY, rows, 128), F32),
        pltpu.VMEM((2, NY, rows, head_v), F32),
        pltpu.VMEM((NY, 2, half, 2 * head_v), BF16),
        pltpu.VMEM((NY, 8, rows), F32),
        pltpu.VMEM((3, 2, half, 2 * head_v), BF16),
        pltpu.VMEM((NY, 8, rows), F32),
        pltpu.VMEM((2, half, 2 * head_v), BF16),
        dma((2, 2)),
        dma((2, 2)),
        dma((2, 2)),
        dma((2, 2)),
        dma((NY,)),
        dma((NY,)),
        pltpu.VMEM((heads, 2, head_v // 2, out_proj.shape[1]), BF16),
        dma((2, 3)),
        dma((2, 3)),
        dma((4, 2)),
        dma((4, 2)),
        pltpu.VMEM((heads, 2, half, head_v), BF16),
        dma((2, 3)),
        dma((2, 3)),
        dma((4, 2)),
        dma((4, 2)),
        pltpu.VMEM((rows, out_proj.shape[1]), BF16),
        dma((out_proj.shape[1] // 256,)),
    ]
    return pl.pallas_call(
        kernel,
        out_shape=jax.ShapeDtypeStruct((rows, out_proj.shape[1]), BF16),
        in_specs=[anywhere] * 6
        + [
            pl.BlockSpec(memory_space=pltpu.SMEM),
            pl.BlockSpec(memory_space=pltpu.VMEM),
            anywhere,
        ],
        out_specs=anywhere,
        scratch_shapes=scratch,
        compiler_params=pltpu.CompilerParams(
            collective_id=0, has_side_effects=True, vmem_limit_bytes=62 * 1024 * 1024
        ),
    )(
        hidden_in, query_one.T, query_two.T, key_one.T, key_two.T, value_proj, lambdas, norm_gain,
        out_proj.reshape(2, head_v // 2, out_proj.shape[1]),
    )


def solution(mesh):
    torus = Mesh(mesh.devices.reshape(NZ, NY, mesh.shape["tp"]), ("sp_0", "sp_1", "tp"))
    placed = (
        P(SP, None),
        P(None, "tp"),
        P(None, "tp"),
        P(None, "tp"),
        P(None, "tp"),
        P(None, "tp"),
        P("tp"),
        P(),
        P("tp", None),
    )
    return jax.shard_map(
        shards, mesh=torus, in_specs=placed, out_specs=P(SP, None), check_vma=False
    )
```

time: 364 us -> 69.5 us (0.19)
  waiting for transfers between devices: 245 us -> 0 us
  Pallas kernels: 0 us -> 66.4 us
  loops' own time: 38.6 us -> 0 us
  local copies, waits for them, and re-layouts: 39.3 us -> 2.3 us
  between operations: 14.2 us -> 0.66 us
  blocking collectives: 12.6 us -> 0 us
  other arithmetic: 6.89 us -> 0 us
  matrix products: 4.87 us -> 0 us
    all_gather x2 -> x0, waiting for transfers between devices: 245 us -> none  [the longest x1 134 us: over_pieces(): parts = lax.all_gather(x, axis).astype(jnp.float32)]
    pallas_call x0 -> x1, Pallas kernels: none -> 66.4 us  [shards(): pl.pallas_call(kernel, out_shape=jax.ShapeDtypeStruct((rows, out_proj.sha...]
    another operation x33 -> x0, loops' own time: 38.6 us -> none  [the longest x1 38.1 us: shards(): lax.scan(absorb_step, softmax_state, (stacked, jnp.arange(block_count, dt...]
    dynamic_slice x32 -> x0, local copies, waits for them, and re-layouts: 17.7 us -> none  [shards(): lax.scan(absorb_step, softmax_state, (stacked, jnp.arange(block_count, dt...]
    unnamed x13 -> x1, local copies, waits for them, and re-layouts: 16 us -> 2.3 us
    all_gather x1 -> x0, blocking collectives: 12.6 us -> none  [whole_of(): nearer = lax.all_gather(x, axes[-1], axis=dim, tiled=True)]
    reduce_sum x3 -> x0, other arithmetic: 6.84 us -> none  [the longest x1 6.39 us: over_pieces(): return parts.sum(axis=0)]
    dot_general x6 -> x0, matrix products: 4.87 us -> none  [the longest x1 2.03 us: shards(): jnp.dot(hidden_in, joined, preferred_element_type=jnp.float32)]
  transfers between devices with their start and end apart: 2 -> 0, of which waited for: 2 -> 0; matrix products, arithmetic and copies ran while one was open for 0% -> 0% of each run, Pallas kernels for 0% -> 0%
where the time goes in v1:
time: 69.5 us; the launch traced here: 69.4 us
  Pallas kernels  66.4 us (96%)
  local copies, waits for them, and re-layouts  2.3 us (3%)
    pallas_call x1, Pallas kernels, shards(): pl.pallas_call(kernel, out_shape=jax.ShapeDtypeStruct((rows, out_proj.sha...  66.4 us
    unnamed x1, local copies, waits for them, and re-layouts  2.3 us

profile of v1, /device:TPU:1, one launch (start us, length us, event | category | flops | bytes accessed | tf_op | source)
XLA Modules:
  0.0 69.4 jit_solution(9909391984885028501)
XLA Ops:
  0.7 66.4 %shard_map.91 = bf16[256,2048]{1,0:T(8,128)(2,1)} custom-call(bf16[256,2048]{1,0:T(8,128)(2,1)} %hidden_hbm.1, bf16[64,2048]{1,0:T(8,128)(2,1)} %bitcast.6, bf16[64,2048]{1,0:T(8,128)(2,1)} %bitcast.7, bf16[64,2048]{1,0:T(8,128)(2,1)} %bitcast.8, bf16[64,2048]{1,0:T(8,128)(2,1)} %bitcast.9, bf16[2048,128]{1,0:T(8,128)(2,1)} %wv_hbm.1, f32[1]{0:T(128)S(6)} %copy.11.lam_ref, ...), custom_call_target="tpu_custom_call" | custom-call | tf_op jit(solution)/shard_map/pallas_call | solution.py:497
  67.1 2.3 %copy.12 = bf16[256,2048]{1,0:T(8,128)(2,1)} copy(bf16[256,2048]{1,0:T(8,128)(2,1)} %shard_map.91) | data formatting | bytes 2097152

commit v2 on v1

v2 whole, which is shorter than its diff:
```python
import math

import jax
import jax.numpy as jnp
from jax import lax
from jax.experimental import pallas as pl
from jax.experimental.pallas import tpu as pltpu
from jax.sharding import Mesh
from jax.sharding import PartitionSpec as P

SP = ("sp_0", "sp_1")
F32 = jnp.float32
BF16 = jnp.bfloat16
MESH = pl.DeviceIdType.MESH

epsilon = 1e-06
masked_score = -1e30

NZ = 16
NY = 4
NX = 4
HALF = NZ // 2
CHUNKS = 4
FAR = 2


def kernel(
    hidden_hbm, wq1_hbm, wq2_hbm, wk1_hbm, wk2_hbm, wv_hbm, lam_hbm, gain_hbm, wo_hbm,
    out_ref,
    hid, wq, wk, wv, lam_ref, gain_ref, load_sem,
    kv, kv_send, kv_recv,
    qbuf, qz, q_send, q_recv,
    m_ref, l_ref, acc_ref,
    opart, stats, orecv, strecv, relay, o_send, o_recv, rel_send, rel_recv, st_send, st_recv,
    wo, wo_send, wo_recv, wo_dsend, wo_drecv,
    nb, nb_send, nb_recv, nb_dsend, nb_drecv,
):
    z = lax.axis_index("sp_0")
    y = lax.axis_index("sp_1")
    t = lax.axis_index("tp")
    x = t // 2
    core = t % 2
    rows = hid.shape[0]
    head_qk = wq.shape[1]
    head_v = wv.shape[1]
    half_rows = rows // 2
    scale = 1.75 * head_qk ** (-0.5) * math.log2(math.e)

    z_up, z_down = (z + 1) % NZ, (z + NZ - 1) % NZ
    y_at = [y, (y + 1) % NY, (y + 2) % NY, (y + 3) % NY]
    x_at = [x, (x + 1) % NX, (x + 2) % NX, (x + 3) % NX]
    tp_at = [2 * xx + core for xx in x_at]
    sibling = 2 * x + (1 - core)

    loads = [
        pltpu.make_async_copy(hidden_hbm, hid, load_sem.at[0]),
        pltpu.make_async_copy(wk1_hbm, wk.at[0], load_sem.at[1]),
        pltpu.make_async_copy(wk2_hbm, wk.at[1], load_sem.at[2]),
        pltpu.make_async_copy(wv_hbm, wv, load_sem.at[3]),
        pltpu.make_async_copy(wq1_hbm, wq.at[0], load_sem.at[4]),
        pltpu.make_async_copy(wq2_hbm, wq.at[1], load_sem.at[5]),
        pltpu.make_async_copy(wo_hbm, wo.at[t], load_sem.at[6]),
        pltpu.make_async_copy(gain_hbm, gain_ref, load_sem.at[7]),
        pltpu.make_async_copy(lam_hbm, lam_ref, load_sem.at[8]),
    ]
    for load in loads:
        load.start()

    barrier = pltpu.get_barrier_semaphore()
    partners = [
        {"sp_0": z_up}, {"sp_0": z_down},
        {"sp_1": y_at[1]}, {"sp_1": y_at[2]}, {"sp_1": y_at[3]},
        {"tp": tp_at[1]}, {"tp": tp_at[3]}, {"tp": sibling},
    ]
    for partner in partners:
        pl.semaphore_signal(barrier, inc=1, device_id=partner, device_id_type=MESH)

    def remote(src, dst, send_sem, recv_sem, device):
        return pltpu.make_async_remote_copy(
            src_ref=src, dst_ref=dst, send_sem=send_sem, recv_sem=recv_sem,
            device_id=device, device_id_type=MESH,
        )

    def dot(a, b, dims=((1,), (0,))):
        return lax.dot_general(a, b, (dims, ((), ())), preferred_element_type=F32)

    with jax.named_scope("load_kv"):
        for load in loads[:4]:
            load.wait()
    with jax.named_scope("proj_kv"):
        h = hid[...]
        k = dot(h, wk[...].reshape(2 * head_qk, wk.shape[2]), ((1,), (1,))).astype(BF16)
        v = dot(h, wv[...]).T.astype(BF16)
        kv[z, 0] = k[:half_rows]
        kv[z, 1] = k[half_rows:]
        kv[z, 2] = v[:, :half_rows]
        kv[z, 3] = v[:, half_rows:]

    with jax.named_scope("entry_barrier"):
        pl.semaphore_wait(barrier, len(partners))

    def up(step, chunk, slot):
        ref = kv.at[slot, chunk]
        return remote(
            ref, ref, kv_send.at[0, step - 1, chunk], kv_recv.at[0, step - 1, chunk], {"sp_0": z_up}
        )

    def down(step, chunk, slot):
        ref = kv.at[slot, chunk]
        return remote(
            ref, ref, kv_send.at[1, step - 1, chunk], kv_recv.at[1, step - 1, chunk], {"sp_0": z_down}
        )

    @pl.when(z < NZ - 1)
    def _():
        for chunk in range(CHUNKS):
            up(1, chunk, z).start()

    @pl.when(z < HALF)
    def _():
        for chunk in range(CHUNKS):
            down(1, chunk, z).start()

    with jax.named_scope("proj_q"):
        loads[4].wait()
        loads[5].wait()
        qbuf[y] = dot(wq[...].reshape(2 * head_qk, wq.shape[2]), h, ((1,), (1,))).astype(BF16)

    def q_copy(off, slot):
        return remote(
            qbuf.at[slot], qbuf.at[slot], q_send.at[off], q_recv.at[off], {"sp_1": y_at[off]}
        )

    for off in (2, 1, 3):
        q_copy(off, y).start()

    def gather_ops(buf, send, recv, dsend, drecv):
        def piece_of(direction, order):
            return direction if order != 1 else 1 - direction

        def hop(direction, order, slot):
            ref = buf.at[slot, piece_of(direction, order)]
            to = tp_at[1] if direction == 0 else tp_at[3]
            return remote(ref, ref, send.at[direction, order], recv.at[direction, order], {"tp": to})

        def across(index, piece, slot):
            ref = buf.at[slot, piece]
            return remote(ref, ref, dsend.at[index, piece], drecv.at[index, piece], {"tp": sibling})

        def came(direction):
            return tp_at[3] if direction == 0 else tp_at[1]

        def start_own():
            for order in range(2):
                for direction in range(2):
                    hop(direction, order, t).start()
            for piece in range(2):
                across(0, piece, t).start()

        def take(order):
            for direction in range(2):
                slot = tp_at[2] if order == 2 else came(direction)
                hop(direction, order, slot).wait_recv()
                if order == 0:
                    hop(direction, 2, slot).start()
                index = 2 if order == 2 else (3 if direction == 0 else 1)
                across(index, piece_of(direction, order), slot).start()

        def take_across():
            for index in range(4):
                slot = 2 * x_at[index] + (1 - core)
                for piece in range(2):
                    across(index, piece, slot).wait_recv()

        def drain():
            for direction in range(2):
                for order in range(3):
                    slot = came(direction) if order == 2 else t
                    hop(direction, order, slot).wait_send()
            for index in range(4):
                for piece in range(2):
                    across(index, piece, tp_at[index]).wait_send()

        return start_own, take, take_across, drain

    wo_start, wo_take, wo_take_across, wo_drain = gather_ops(wo, wo_send, wo_recv, wo_dsend, wo_drecv)
    nb_start, nb_take, nb_take_across, nb_drain = gather_ops(nb, nb_send, nb_recv, nb_dsend, nb_drecv)

    loads[6].wait()
    wo_start()

    def pass_on(step, chunk):
        low, high = (z + NZ - step) % NZ, (z + step) % NZ

        @pl.when(z >= step)
        def _():
            up(step, chunk, low).wait_recv()

            @pl.when((z < NZ - 1) & ((step < HALF - 1) | (chunk < CHUNKS // 2)))
            def _():
                up(step + 1, chunk, low).start()

        @pl.when(high < HALF)
        def _():
            down(step, chunk, high).wait_recv()

            @pl.when((step < HALF - 1) | (chunk >= CHUNKS // 2))
            def _():
                down(step + 1, chunk, high).start()

    with jax.named_scope("first_pass"):
        for chunk in range(CHUNKS):
            pass_on(1, chunk)

    with jax.named_scope("wait_q"):
        for off in (1, 3, 2):
            q_copy(off, y_at[(NY - off) % NY]).wait_recv()

    def split_queries(block, _):
        q = qbuf[block].astype(F32) * scale
        high = q.astype(BF16)
        low = (q - high.astype(F32)).astype(BF16)
        nothing = jnp.zeros((head_qk, rows), BF16)
        qz[0, block] = jnp.concatenate((high[:head_qk], nothing, low[:head_qk], nothing), axis=0)
        qz[1, block] = jnp.concatenate((nothing, high[head_qk:], nothing, low[head_qk:]), axis=0)
        return 0

    with jax.named_scope("split_q"):
        lax.fori_loop(0, NY, split_queries, 0)

    def block_of(slot):
        keys = jnp.concatenate((kv[slot, 0], kv[slot, 1]), axis=0)
        return (
            jnp.concatenate((keys, keys), axis=1),
            jnp.concatenate((kv[slot, 2], kv[slot, 3]), axis=1),
        )

    def attend(blocks, slots, own=False):
        keys, vals = zip(*[block_of(slot) for slot in slots])
        vals = jnp.concatenate(vals, axis=1)
        units = [(pick, block) for block in blocks for pick in range(2)]
        groups = rows // 8

        def allowed(block):
            k_pos = y * rows + lax.broadcasted_iota(jnp.int32, (rows, rows), 0)
            q_pos = block * rows + lax.broadcasted_iota(jnp.int32, (rows, rows), 1)
            return k_pos <= q_pos

        def score(unit):
            pick, block = unit
            found = [dot(one, qz[pick, block]) for one in keys]
            if own:
                found = [jnp.where(allowed(block), one, masked_score) for one in found]
            highest = None
            for one in found:
                top = jnp.max(one.reshape(groups, 8, rows), axis=0)
                highest = top if highest is None else jnp.maximum(highest, top)
            return found, highest

        def absorb(unit, found, highest):
            pick, block = unit
            now = jnp.broadcast_to(jnp.max(highest, axis=0, keepdims=True), (8, rows))
            if not own:
                before = m_ref[pick, block]
                now = jnp.maximum(before, now)
                rescale = jnp.exp2(before - now)
            total = None
            parts = []
            for one in found:
                part = jnp.exp2(one.reshape(groups, 8, rows) - now[None])
                if own:
                    part = jnp.where(allowed(block).reshape(groups, 8, rows), part, 0.0)
                summed = jnp.sum(part, axis=0)
                total = summed if total is None else total + summed
                parts.append(part.reshape(rows, rows).astype(BF16))
            added = dot(vals, jnp.concatenate(parts, axis=0))
            m_ref[pick, block] = now
            if own:
                l_ref[pick, block] = total
                acc_ref[pick, block] = added
            else:
                l_ref[pick, block] = l_ref[pick, block] * rescale + total
                kept = acc_ref[pick, block].reshape(head_v // 8, 8, rows) * rescale[None]
                acc_ref[pick, block] = kept.reshape(head_v, rows) + added

        ahead = score(units[0])
        for index, unit in enumerate(units):
            here = ahead
            if index + 1 < len(units):
                ahead = score(units[index + 1])
            absorb(unit, *here)

    def attend_pair(step, part):
        low, high = (z + NZ - step) % NZ, (z + step) % NZ
        blocks = (2 * part, 2 * part + 1)

        @pl.when(z >= NZ - step)
        def _():
            attend(blocks, (low, high))

        @pl.when((z >= step) & (z < NZ - step))
        def _():
            attend(blocks, (low,))

    opposite = (z + HALF) % NZ

    def o_copy(direction, piece, slot):
        to = y_at[1] if direction == 0 else y_at[3]
        return remote(
            opart.at[slot, piece], orecv.at[direction, piece],
            o_send.at[direction, piece], o_recv.at[direction, piece], {"sp_1": to},
        )

    def rel_copy(direction, slot):
        to = y_at[1] if direction == 0 else y_at[3]
        return remote(
            opart.at[slot, direction], relay.at[direction],
            rel_send.at[direction, 0], rel_recv.at[direction, 0], {"sp_1": to},
        )

    def rel_forward(direction):
        to = y_at[1] if direction == 0 else y_at[3]
        return remote(
            relay.at[direction], orecv.at[2, direction],
            rel_send.at[direction, 1], rel_recv.at[direction, 1], {"sp_1": to},
        )

    def st_copy(off, slot):
        return remote(
            stats.at[slot], strecv.at[off], st_send.at[off], st_recv.at[off], {"sp_1": y_at[off]}
        )

    def pack(block):
        table = []
        for pick in range(2):
            table.append(m_ref[pick, block][:1])
            table.append(jnp.sum(l_ref[pick, block], axis=0, keepdims=True))
            part = acc_ref[pick, block].astype(BF16)
            for piece in range(2):
                span = slice(piece * half_rows, (piece + 1) * half_rows)
                opart[block, piece, pick * head_v : (pick + 1) * head_v] = part[:, span]
        table.append(jnp.zeros((4, rows), F32))
        stats[block] = jnp.concatenate(table, axis=0)

    def finish_send(late):
        if late:

            @pl.when(z >= HALF)
            def _():
                attend((y_at[2], y_at[1]), (opposite,))

        pack(y_at[2])
        rel_copy(0, y_at[2]).start()
        rel_copy(1, y_at[2]).start()
        st_copy(2, y_at[2]).start()
        pack(y_at[1])
        o_copy(0, 0, y_at[1]).start()
        o_copy(0, 1, y_at[1]).start()
        st_copy(1, y_at[1]).start()
        if late:

            @pl.when(z >= HALF)
            def _():
                attend((y_at[3], y_at[0]), (opposite,))

        pack(y_at[3])
        o_copy(1, 0, y_at[3]).start()
        o_copy(1, 1, y_at[3]).start()
        st_copy(3, y_at[3]).start()
        pack(y_at[0])

    def finish_relay():
        for direction in range(2):
            rel_copy(direction, y_at[2]).wait_recv()
            rel_forward(direction).start()

    def finish_combine():
        for off in range(1, NY):
            st_copy(off, y_at[0]).wait_recv()
        lam = lam_ref[0]
        tables = [stats[y], strecv[1], strecv[3], strecv[2]]
        coefs = []
        for pick in range(2):
            maxima = [table[2 * pick : 2 * pick + 1] for table in tables]
            sums = [table[2 * pick + 1 : 2 * pick + 2] for table in tables]
            highest = maxima[0]
            for other in maxima[1:]:
                highest = jnp.maximum(highest, other)
            shares = [jnp.exp2(one - highest) for one in maxima]
            total = shares[0] * sums[0]
            for share, one in zip(shares[1:], sums[1:]):
                total = total + share * one
            factor = (1.0 if pick == 0 else -lam) / total
            coefs.append([share * factor for share in shares])
        gain = gain_ref[...].reshape(1, head_v)
        for piece in range(2):
            o_copy(0, piece, y_at[1]).wait_recv()
            o_copy(1, piece, y_at[3]).wait_recv()
            rel_forward(piece).wait_recv()
            span = slice(piece * half_rows, (piece + 1) * half_rows)
            mixed = None
            for pick in range(2):
                parts = [acc_ref[pick, y][:, span]]
                for source in range(3):
                    one = orecv[source, piece, pick * head_v : (pick + 1) * head_v]
                    parts.append(one.astype(F32))
                for part, coef in zip(parts, coefs[pick]):
                    term = part * coef[:, span]
                    mixed = term if mixed is None else mixed + term
            spread = lax.rsqrt(jnp.mean(mixed * mixed, axis=0, keepdims=True) + epsilon)
            nb[t, piece] = ((mixed * spread).T * gain).astype(BF16)
        nb_start()

    def finish_gather():
        nb_take(0)
        nb_take(1)
        nb_take(2)

    loads[7].wait()
    loads[8].wait()

    def ring_step(index, _):
        step, part = index // 2, index % 2

        def pass_one(chunk):
            @pl.when(step < HALF)
            def _():
                with jax.named_scope("pass_on"):
                    pass_on(step, chunk)

        pass_one(2 * part)

        @pl.when(step == 2)
        def _():
            attend((2 * part, 2 * part + 1), (z,), own=True)

        pass_one(2 * part + 1)
        with jax.named_scope("attend_pair"):
            attend_pair(step - 1, part)

        @pl.when(index == 8)
        def _():
            wo_take(0)

        @pl.when(index == 12)
        def _():
            wo_take(1)

        for at, phase in ((5, lambda: finish_send(False)), (7, finish_relay), (10, finish_combine), (14, finish_gather)):

            @pl.when((z == 0) & (index == at))
            def _(phase=phase):
                phase()

        return 0

    with jax.named_scope("ring"):
        lax.fori_loop(4, 2 * HALF + 2, ring_step, 0)

    with jax.named_scope("last_wait"):

        @pl.when(z >= HALF)
        def _():
            for chunk in range(CHUNKS):
                if chunk < CHUNKS // 2:
                    up(HALF, chunk, opposite).wait_recv()
                else:
                    down(HALF, chunk, opposite).wait_recv()

    @pl.when(z > 0)
    def _():
        with jax.named_scope("finish_send"):
            finish_send(True)
        with jax.named_scope("finish_relay"):
            finish_relay()

    with jax.named_scope("wo_far"):
        wo_take(2)

    @pl.when(z > 0)
    def _():
        with jax.named_scope("finish_combine"):
            finish_combine()
        with jax.named_scope("finish_gather"):
            finish_gather()

    with jax.named_scope("take_across"):
        wo_take_across()
        nb_take_across()

    with jax.named_scope("out_proj"):
        lhs = jnp.concatenate([nb[head].reshape(rows, head_v) for head in range(2 * NX)], axis=1)
        width = 256
        for left in range(0, out_ref.shape[1], width):
            rhs = wo[:, :, :, left : left + width].reshape(2 * NX * head_v, width)
            out_ref[:, left : left + width] = dot(lhs, rhs).astype(BF16)

    def drain_ring(index, _):
        step, chunk = index // CHUNKS, index % CHUNKS

        @pl.when((z < NZ - 1) & (z + 1 >= step) & ((step < HALF) | (chunk < CHUNKS // 2)))
        def _():
            up(step, chunk, z).wait_send()

        @pl.when(((z + step - 1) % NZ < HALF) & ((step < HALF) | (chunk >= CHUNKS // 2)))
        def _():
            down(step, chunk, z).wait_send()

        return 0

    with jax.named_scope("drain"):
        lax.fori_loop(CHUNKS, (HALF + 1) * CHUNKS, drain_ring, 0)
        for off in range(1, NY):
            q_copy(off, y).wait_send()
            st_copy(off, y).wait_send()
        for direction in range(2):
            for piece in range(2):
                o_copy(direction, piece, y).wait_send()
            rel_copy(direction, y).wait_send()
            rel_forward(direction).wait_send()
        wo_drain()
        nb_drain()


def shards(
    hidden_in, query_one, query_two, key_one, key_two, value_proj, lambdas, norm_gain, out_proj
):
    rows, depth = hidden_in.shape
    head_qk = query_one.shape[1]
    head_v = value_proj.shape[1]
    half = rows // 2
    heads = 2 * NX
    dma = pltpu.SemaphoreType.DMA
    scratch = [
        pltpu.VMEM((rows, depth), BF16),
        pltpu.VMEM((2, head_qk, depth), BF16),
        pltpu.VMEM((2, head_qk, depth), BF16),
        pltpu.VMEM((depth, head_v), BF16),
        pltpu.SMEM((1,), F32),
        pltpu.VMEM((head_v,), F32),
        dma((9,)),
        pltpu.VMEM((NZ, CHUNKS, half, head_v), BF16),
        dma((2, HALF, CHUNKS)),
        dma((2, HALF, CHUNKS)),
        pltpu.VMEM((NY, 2 * head_qk, rows), BF16),
        pltpu.VMEM((2, NY, 4 * head_qk, rows), BF16),
        dma((NY,)),
        dma((NY,)),
        pltpu.VMEM((2, NY, 8, rows), F32),
        pltpu.VMEM((2, NY, 8, rows), F32),
        pltpu.VMEM((2, NY, head_v, rows), F32),
        pltpu.VMEM((NY, 2, 2 * head_v, half), BF16),
        pltpu.VMEM((NY, 8, rows), F32),
        pltpu.VMEM((3, 2, 2 * head_v, half), BF16),
        pltpu.VMEM((NY, 8, rows), F32),
        pltpu.VMEM((2, 2 * head_v, half), BF16),
        dma((2, 2)),
        dma((2, 2)),
        dma((2, 2)),
        dma((2, 2)),
        dma((NY,)),
        dma((NY,)),
        pltpu.VMEM((heads, 2, head_v // 2, out_proj.shape[1]), BF16),
        dma((2, 3)),
        dma((2, 3)),
        dma((4, 2)),
        dma((4, 2)),
        pltpu.VMEM((heads, 2, half, head_v), BF16),
        dma((2, 3)),
        dma((2, 3)),
        dma((4, 2)),
        dma((4, 2)),
    ]
    return pl.pallas_call(
        kernel,
        out_shape=pltpu.VMEM((rows, out_proj.shape[1]), BF16),
        in_specs=[pl.BlockSpec(memory_space=pltpu.HBM)] * 9,
        out_specs=pl.BlockSpec(memory_space=pltpu.VMEM),
        scratch_shapes=scratch,
        compiler_params=pltpu.CompilerParams(
            collective_id=0, has_side_effects=True, vmem_limit_bytes=60 * 1024 * 1024
        ),
    )(
        hidden_in, query_one.T, query_two.T, key_one.T, key_two.T, value_proj, lambdas, norm_gain,
        out_proj.reshape(2, head_v // 2, out_proj.shape[1]),
    )


def solution(mesh):
    torus = Mesh(mesh.devices.reshape(NZ, NY, mesh.shape["tp"]), ("sp_0", "sp_1", "tp"))
    placed = (
        P(SP, None),
        P(None, "tp"),
        P(None, "tp"),
        P(None, "tp"),
        P(None, "tp"),
        P(None, "tp"),
        P("tp"),
        P(),
        P("tp", None),
    )
    return jax.shard_map(
        shards, mesh=torus, in_specs=placed, out_specs=P(SP, None), check_vma=False
    )
```

time: 69.5 us -> 57.2 us (0.82)
  the two profiles are of different devices: /device:TPU:1 before, /device:TPU:385 now
where the time goes in v2:
time: 57.2 us; the launch traced here: 57.1 us
  Pallas kernels  55.4 us (97%)
  local copies, waits for them, and re-layouts  0.97 us (2%)
  between operations  0.66 us (1%)
    pallas_call x1, Pallas kernels, shards(): pl.pallas_call(kernel, out_shape=pltpu.VMEM((rows, out_proj.shape[1]), BF...  55.4 us

profile of v2, /device:TPU:385, one launch (start us, length us, event | category | flops | bytes accessed | tf_op | source)
XLA Modules:
  0.0 57.1 jit_solution(3662953325723680693)
XLA Ops:
  0.7 55.4 %shard_map.91 = bf16[256,2048]{1,0:T(8,128)(2,1)S(1)} custom-call(bf16[256,2048]{1,0:T(8,128)(2,1)} %hidden_hbm.1, bf16[64,2048]{1,0:T(8,128)(2,1)} %bitcast.6, bf16[64,2048]{1,0:T(8,128)(2,1)} %bitcast.7, bf16[64,2048]{1,0:T(8,128)(2,1)} %bitcast.8, bf16[64,2048]{1,0:T(8,128)(2,1)} %bitcast.9, bf16[2048,128]{1,0:T(8,128)(2,1)} %wv_hbm.1, ...), custom_call_target="tpu_custom_call" | custom-call | tf_op jit(solution)/shard_map/pallas_call | solution.py:574
  56.1 1.0 %copy.11 = bf16[256,2048]{1,0:T(8,128)(2,1)} copy(bf16[256,2048]{1,0:T(8,128)(2,1)S(1)} %shard_map.91) | data formatting | bytes 2097152

commit v3 on v2

--- a/solution.py
+++ b/solution.py
@@ -28,12 +28,13 @@
     hidden_hbm, wq1_hbm, wq2_hbm, wk1_hbm, wk2_hbm, wv_hbm, lam_hbm, gain_hbm, wo_hbm,
     out_ref,
     hid, wq, wk, wv, lam_ref, gain_ref, load_sem,
-    kv, kv_send, kv_recv,
+    kv, kv_send, kv_recv, own_send, own_recv, give_send, give_recv,
     qbuf, qz, q_send, q_recv,
     m_ref, l_ref, acc_ref,
     opart, stats, orecv, strecv, relay, o_send, o_recv, rel_send, rel_recv, st_send, st_recv,
     wo, wo_send, wo_recv, wo_dsend, wo_drecv,
     nb, nb_send, nb_recv, nb_dsend, nb_drecv,
+    out_v, out_sem,
 ):
     z = lax.axis_index("sp_0")
     y = lax.axis_index("sp_1")
@@ -91,10 +92,8 @@
         h = hid[...]
         k = dot(h, wk[...].reshape(2 * head_qk, wk.shape[2]), ((1,), (1,))).astype(BF16)
         v = dot(h, wv[...]).T.astype(BF16)
-        kv[z, 0] = k[:half_rows]
-        kv[z, 1] = k[half_rows:]
-        kv[z, 2] = v[:, :half_rows]
-        kv[z, 3] = v[:, half_rows:]
+        for chunk, piece in enumerate((k[:half_rows], k[half_rows:], v[:, :half_rows], v[:, half_rows:])):
+            kv[z, chunk, core] = piece
 
     with jax.named_scope("entry_barrier"):
         pl.semaphore_wait(barrier, len(partners))
@@ -111,15 +110,21 @@
             ref, ref, kv_send.at[1, step - 1, chunk], kv_recv.at[1, step - 1, chunk], {"sp_0": z_down}
         )
 
-    @pl.when(z < NZ - 1)
+    def own_over(chunk):
+        ref = kv.at[z, chunk, 0]
+        return remote(ref, ref, own_send.at[chunk], own_recv.at[chunk], {"tp": sibling})
+
+    def give(direction, step, chunk, slot):
+        ref = kv.at[slot, chunk, 0]
+        return remote(
+            ref, ref, give_send.at[direction, step - 1, chunk], give_recv.at[direction, step - 1, chunk],
+            {"tp": sibling},
+        )
+
+    @pl.when(core == 0)
     def _():
         for chunk in range(CHUNKS):
-            up(1, chunk, z).start()
-
-    @pl.when(z < HALF)
-    def _():
-        for chunk in range(CHUNKS):
-            down(1, chunk, z).start()
+            own_over(chunk).start()
 
     with jax.named_scope("proj_q"):
         loads[4].wait()
@@ -133,6 +138,20 @@
 
     for off in (2, 1, 3):
         q_copy(off, y).start()
+
+    @pl.when(core == 1)
+    def _():
+        for chunk in range(CHUNKS):
+            own_over(chunk).wait_recv()
+
+            @pl.when(z < NZ - 1)
+            def _(chunk=chunk):
+                up(1, chunk, z).start()
+
+            @pl.when(z < HALF)
+            def _(chunk=chunk):
+                down(1, chunk, z).start()
+
 
     def gather_ops(buf, send, recv, dsend, drecv):
         def piece_of(direction, order):
@@ -184,7 +203,67 @@
         return start_own, take, take_across, drain
 
     wo_start, wo_take, wo_take_across, wo_drain = gather_ops(wo, wo_send, wo_recv, wo_dsend, wo_drecv)
-    nb_start, nb_take, nb_take_across, nb_drain = gather_ops(nb, nb_send, nb_recv, nb_dsend, nb_drecv)
+
+    def nb_hop(direction, order, head, chip):
+        piece = direction if order != 1 else 1 - direction
+        ref = nb.at[2 * chip + head, piece]
+        to = 2 * (x_at[1] if direction == 0 else x_at[3]) + 1
+        return remote(
+            ref, ref, nb_send.at[direction, order, head], nb_recv.at[direction, order, head], {"tp": to}
+        )
+
+    def nb_across(index, head, piece, chip):
+        ref = nb.at[2 * chip + head, piece]
+        return remote(
+            ref, ref, nb_dsend.at[index, head, piece], nb_drecv.at[index, head, piece], {"tp": sibling}
+        )
+
+    def nb_start():
+        for piece in range(2):
+            nb_across(0, core, piece, x).start()
+
+    def nb_gather():
+        @pl.when(core == 1)
+        def _():
+            for head in (1, 0):
+                for order in range(2):
+                    for direction in range(2):
+                        piece = direction if order != 1 else 1 - direction
+                        if head == 0 and order == 0:
+                            nb_across(0, 0, piece, x).wait_recv()
+                        nb_hop(direction, order, head, x).start()
+            for head in (1, 0):
+                for order in range(3):
+                    for direction in range(2):
+                        piece = direction if order != 1 else 1 - direction
+                        index = 2 if order == 2 else (3 if direction == 0 else 1)
+                        nb_hop(direction, order, head, x_at[index]).wait_recv()
+                        if order == 0:
+                            nb_hop(direction, 2, head, x_at[index]).start()
+                        nb_across(index, head, piece, x_at[index]).start()
+
+        @pl.when(core == 0)
+        def _():
+            nb_across(0, 1, 0, x).wait_recv()
+            nb_across(0, 1, 1, x).wait_recv()
+            for head in (1, 0):
+                for index in (1, 3, 2):
+                    for piece in range(2):
+                        nb_across(index, head, piece, x_at[index]).wait_recv()
+
+    def nb_drain():
+        for piece in range(2):
+            nb_across(0, core, piece, x).wait_send()
+
+        @pl.when(core == 1)
+        def _():
+            for head in (1, 0):
+                for direction in range(2):
+                    for order in range(3):
+                        nb_hop(direction, order, head, x).wait_send()
+                for index in (1, 3, 2):
+                    for piece in range(2):
+                        nb_across(index, head, piece, x).wait_send()
 
     loads[6].wait()
     wo_start()
@@ -192,21 +271,39 @@
     def pass_on(step, chunk):
         low, high = (z + NZ - step) % NZ, (z + step) % NZ
 
-        @pl.when(z >= step)
-        def _():
-            up(step, chunk, low).wait_recv()
-
-            @pl.when((z < NZ - 1) & ((step < HALF - 1) | (chunk < CHUNKS // 2)))
+        @pl.when(core == 1)
+        def _():
+            @pl.when(z >= step)
             def _():
-                up(step + 1, chunk, low).start()
-
-        @pl.when(high < HALF)
-        def _():
-            down(step, chunk, high).wait_recv()
-
-            @pl.when((step < HALF - 1) | (chunk >= CHUNKS // 2))
+                up(step, chunk, low).wait_recv()
+
+                @pl.when((z < NZ - 1) & ((step < HALF - 1) | (chunk < CHUNKS // 2)))
+                def _():
+                    up(step + 1, chunk, low).start()
+
+                give(0, step, chunk, low).start()
+
+            @pl.when(high < HALF)
             def _():
-                down(step + 1, chunk, high).start()
+                down(step, chunk, high).wait_recv()
+
+                @pl.when((step < HALF - 1) | (chunk >= CHUNKS // 2))
+                def _():
+                    down(step + 1, chunk, high).start()
+
+                @pl.when(z >= NZ - step)
+                def _():
+                    give(1, step, chunk, high).start()
+
+        @pl.when(core == 0)
+        def _():
+            @pl.when(z >= step)
+            def _():
+                give(0, step, chunk, low).wait_recv()
+
+            @pl.when(z >= NZ - step)
+            def _():
+                give(1, step, chunk, high).wait_recv()
 
     with jax.named_scope("first_pass"):
         for chunk in range(CHUNKS):
@@ -229,10 +326,10 @@
         lax.fori_loop(0, NY, split_queries, 0)
 
     def block_of(slot):
-        keys = jnp.concatenate((kv[slot, 0], kv[slot, 1]), axis=0)
+        keys = jnp.concatenate((kv[slot, 0, core], kv[slot, 1, core]), axis=0)
         return (
             jnp.concatenate((keys, keys), axis=1),
-            jnp.concatenate((kv[slot, 2], kv[slot, 3]), axis=1),
+            jnp.concatenate((kv[slot, 2, core], kv[slot, 3, core]), axis=1),
         )
 
     def attend(blocks, slots, own=False):
@@ -412,9 +509,7 @@
         nb_start()
 
     def finish_gather():
-        nb_take(0)
-        nb_take(1)
-        nb_take(2)
+        nb_gather()
 
     loads[7].wait()
     loads[8].wait()
@@ -462,15 +557,61 @@
         @pl.when(z >= HALF)
         def _():
             for chunk in range(CHUNKS):
-                if chunk < CHUNKS // 2:
-                    up(HALF, chunk, opposite).wait_recv()
-                else:
-                    down(HALF, chunk, opposite).wait_recv()
+                direction = 0 if chunk < CHUNKS // 2 else 1
+                last = (up, down)[direction](HALF, chunk, opposite)
+                handed = give(direction, HALF, chunk, opposite)
+
+                @pl.when(core == 1)
+                def _(last=last, handed=handed):
+                    last.wait_recv()
+                    handed.start()
+
+                @pl.when(core == 0)
+                def _(handed=handed):
+                    handed.wait_recv()
 
     @pl.when(z > 0)
     def _():
         with jax.named_scope("finish_send"):
             finish_send(True)
+
+    def drain_ring(index, _):
+        step, chunk = index // CHUNKS, index % CHUNKS
+
+        @pl.when((z < NZ - 1) & (z + 1 >= step) & ((step < HALF) | (chunk < CHUNKS // 2)))
+        def _():
+            up(step, chunk, z).wait_send()
+
+        @pl.when(((z + step - 1) % NZ < HALF) & ((step < HALF) | (chunk >= CHUNKS // 2)))
+        def _():
+            down(step, chunk, z).wait_send()
+
+        @pl.when((z >= step) & ((step < HALF) | (chunk < CHUNKS // 2)))
+        def _():
+            give(0, step, chunk, z).wait_send()
+
+        @pl.when((z >= NZ - step) & ((step < HALF) | (chunk >= CHUNKS // 2)))
+        def _():
+            give(1, step, chunk, z).wait_send()
+
+        return 0
+
+    with jax.named_scope("drain_ring"):
+
+        @pl.when(core == 1)
+        def _():
+            lax.fori_loop(CHUNKS, (HALF + 1) * CHUNKS, drain_ring, 0)
+
+        @pl.when(core == 0)
+        def _():
+            for chunk in range(CHUNKS):
+                own_over(chunk).wait_send()
+
+        for off in range(1, NY):
+            q_copy(off, y).wait_send()
+
+    @pl.when(z > 0)
+    def _():
         with jax.named_scope("finish_relay"):
             finish_relay()
 
@@ -481,43 +622,40 @@
     def _():
         with jax.named_scope("finish_combine"):
             finish_combine()
-        with jax.named_scope("finish_gather"):
-            finish_gather()
-
-    with jax.named_scope("take_across"):
-        wo_take_across()
-        nb_take_across()
-
-    with jax.named_scope("out_proj"):
-        lhs = jnp.concatenate([nb[head].reshape(rows, head_v) for head in range(2 * NX)], axis=1)
-        width = 256
-        for left in range(0, out_ref.shape[1], width):
-            rhs = wo[:, :, :, left : left + width].reshape(2 * NX * head_v, width)
-            out_ref[:, left : left + width] = dot(lhs, rhs).astype(BF16)
-
-    def drain_ring(index, _):
-        step, chunk = index // CHUNKS, index % CHUNKS
-
-        @pl.when((z < NZ - 1) & (z + 1 >= step) & ((step < HALF) | (chunk < CHUNKS // 2)))
-        def _():
-            up(step, chunk, z).wait_send()
-
-        @pl.when(((z + step - 1) % NZ < HALF) & ((step < HALF) | (chunk >= CHUNKS // 2)))
-        def _():
-            down(step, chunk, z).wait_send()
-
-        return 0
-
-    with jax.named_scope("drain"):
-        lax.fori_loop(CHUNKS, (HALF + 1) * CHUNKS, drain_ring, 0)
+    with jax.named_scope("drain_parts"):
         for off in range(1, NY):
-            q_copy(off, y).wait_send()
             st_copy(off, y).wait_send()
         for direction in range(2):
             for piece in range(2):
                 o_copy(direction, piece, y).wait_send()
             rel_copy(direction, y).wait_send()
             rel_forward(direction).wait_send()
+
+    @pl.when(z > 0)
+    def _():
+        with jax.named_scope("finish_gather"):
+            finish_gather()
+
+    with jax.named_scope("take_across"):
+        wo_take_across()
+
+    with jax.named_scope("out_proj"):
+        lhs = jnp.concatenate([nb[head].reshape(rows, head_v) for head in range(2 * NX)], axis=1)
+        width = 256
+        tiles = []
+        for left in range(0, out_ref.shape[1], width):
+            rhs = wo[:, :, :, left : left + width].reshape(2 * NX * head_v, width)
+            out_v[:, left : left + width] = dot(lhs, rhs).astype(BF16)
+            tile = pltpu.make_async_copy(
+                out_v.at[:, left : left + width], out_ref.at[:, left : left + width],
+                out_sem.at[left // width],
+            )
+            tile.start()
+            tiles.append(tile)
+
+    with jax.named_scope("drain"):
+        for tile in tiles:
+            tile.wait()
         wo_drain()
         nb_drain()
 
@@ -539,7 +677,11 @@
         pltpu.SMEM((1,), F32),
         pltpu.VMEM((head_v,), F32),
         dma((9,)),
-        pltpu.VMEM((NZ, CHUNKS, half, head_v), BF16),
+        pltpu.VMEM((NZ, CHUNKS, 2, half, head_v), BF16),
+        dma((2, HALF, CHUNKS)),
+        dma((2, HALF, CHUNKS)),
+        dma((CHUNKS,)),
+        dma((CHUNKS,)),
         dma((2, HALF, CHUNKS)),
         dma((2, HALF, CHUNKS)),
         pltpu.VMEM((NY, 2 * head_qk, rows), BF16),
@@ -566,16 +708,18 @@
         dma((4, 2)),
         dma((4, 2)),
         pltpu.VMEM((heads, 2, half, head_v), BF16),
-        dma((2, 3)),
-        dma((2, 3)),
-        dma((4, 2)),
-        dma((4, 2)),
+        dma((2, 3, 2)),
+        dma((2, 3, 2)),
+        dma((4, 2, 2)),
+        dma((4, 2, 2)),
+        pltpu.VMEM((rows, out_proj.shape[1]), BF16),
+        dma((out_proj.shape[1] // 256,)),
     ]
     return pl.pallas_call(
         kernel,
         out_shape=pltpu.VMEM((rows, out_proj.shape[1]), BF16),
         in_specs=[pl.BlockSpec(memory_space=pltpu.HBM)] * 9,
-        out_specs=pl.BlockSpec(memory_space=pltpu.VMEM),
+        out_specs=pl.BlockSpec(memory_space=pl.ANY),
         scratch_shapes=scratch,
         compiler_params=pltpu.CompilerParams(
             collective_id=0, has_side_effects=True, vmem_limit_bytes=60 * 1024 * 1024

time: 57.2 us -> 64.5 us (1.13)
  the two profiles are of different devices: /device:TPU:385 before, /device:TPU:480 now
where the time goes in v3:
time: 64.5 us; the launch traced here: 64.4 us
  Pallas kernels  62.8 us (97%)
  local copies, waits for them, and re-layouts  0.97 us (2%)
  between operations  0.66 us (1%)
    pallas_call x1, Pallas kernels, shards(): pl.pallas_call(kernel, out_shape=pltpu.VMEM((rows, out_proj.shape[1]), BF...  62.8 us

profile of v3, /device:TPU:480, one launch (start us, length us, event | category | flops | bytes accessed | tf_op | source)
XLA Modules:
  0.0 64.4 jit_solution(2286538929881989837)
XLA Ops:
  0.7 62.8 %shard_map.91 = bf16[256,2048]{1,0:T(8,128)(2,1)S(1)} custom-call(bf16[256,2048]{1,0:T(8,128)(2,1)} %hidden_hbm.1, bf16[64,2048]{1,0:T(8,128)(2,1)} %bitcast.6, bf16[64,2048]{1,0:T(8,128)(2,1)} %bitcast.7, bf16[64,2048]{1,0:T(8,128)(2,1)} %bitcast.8, bf16[64,2048]{1,0:T(8,128)(2,1)} %bitcast.9, bf16[2048,128]{1,0:T(8,128)(2,1)} %wv_hbm.1, ...), custom_call_target="tpu_custom_call" | custom-call | tf_op jit(solution)/shard_map/pallas_call | solution.py:718
  63.4 1.0 %copy.11 = bf16[256,2048]{1,0:T(8,128)(2,1)} copy(bf16[256,2048]{1,0:T(8,128)(2,1)S(1)} %shard_map.91) | data formatting | bytes 2097152

commit v4 on v2

--- a/solution.py
+++ b/solution.py
@@ -30,8 +30,8 @@
     hid, wq, wk, wv, lam_ref, gain_ref, load_sem,
     kv, kv_send, kv_recv,
     qbuf, qz, q_send, q_recv,
-    m_ref, l_ref, acc_ref,
-    opart, stats, orecv, strecv, relay, o_send, o_recv, rel_send, rel_recv, st_send, st_recv,
+    m_ref, l_ref, acc_ref, ahead_ref, ahead_max,
+    opart, stats, orecv, strecv, relay, o_send, o_recv, rel_recv, st_send, st_recv,
     wo, wo_send, wo_recv, wo_dsend, wo_drecv,
     nb, nb_send, nb_recv, nb_dsend, nb_drecv,
 ):
@@ -70,7 +70,7 @@
     partners = [
         {"sp_0": z_up}, {"sp_0": z_down},
         {"sp_1": y_at[1]}, {"sp_1": y_at[2]}, {"sp_1": y_at[3]},
-        {"tp": tp_at[1]}, {"tp": tp_at[3]}, {"tp": sibling},
+        {"tp": tp_at[1]}, {"tp": tp_at[2]}, {"tp": tp_at[3]}, {"tp": sibling},
     ]
     for partner in partners:
         pl.semaphore_signal(barrier, inc=1, device_id=partner, device_id_type=MESH)
@@ -102,13 +102,13 @@
     def up(step, chunk, slot):
         ref = kv.at[slot, chunk]
         return remote(
-            ref, ref, kv_send.at[0, step - 1, chunk], kv_recv.at[0, step - 1, chunk], {"sp_0": z_up}
+            ref, ref, kv_send.at[0, chunk], kv_recv.at[0, step - 1, chunk], {"sp_0": z_up}
         )
 
     def down(step, chunk, slot):
         ref = kv.at[slot, chunk]
         return remote(
-            ref, ref, kv_send.at[1, step - 1, chunk], kv_recv.at[1, step - 1, chunk], {"sp_0": z_down}
+            ref, ref, kv_send.at[1, chunk], kv_recv.at[1, step - 1, chunk], {"sp_0": z_down}
         )
 
     @pl.when(z < NZ - 1)
@@ -128,8 +128,11 @@
 
     def q_copy(off, slot):
         return remote(
-            qbuf.at[slot], qbuf.at[slot], q_send.at[off], q_recv.at[off], {"sp_1": y_at[off]}
-        )
+            qbuf.at[slot], qbuf.at[slot], q_send.at[0], q_recv.at[0], {"sp_1": y_at[off]}
+        )
+
+    def all_of(ref, send_sem, recv_sem):
+        return remote(ref, ref, send_sem, recv_sem, {"tp": sibling})
 
     for off in (2, 1, 3):
         q_copy(off, y).start()
@@ -141,11 +144,11 @@
         def hop(direction, order, slot):
             ref = buf.at[slot, piece_of(direction, order)]
             to = tp_at[1] if direction == 0 else tp_at[3]
-            return remote(ref, ref, send.at[direction, order], recv.at[direction, order], {"tp": to})
-
-        def across(index, piece, slot):
+            return remote(ref, ref, send.at[0], recv.at[order], {"tp": to})
+
+        def across(piece, slot):
             ref = buf.at[slot, piece]
-            return remote(ref, ref, dsend.at[index, piece], drecv.at[index, piece], {"tp": sibling})
+            return remote(ref, ref, dsend.at[0], drecv.at[0], {"tp": sibling})
 
         def came(direction):
             return tp_at[3] if direction == 0 else tp_at[1]
@@ -155,36 +158,45 @@
                 for direction in range(2):
                     hop(direction, order, t).start()
             for piece in range(2):
-                across(0, piece, t).start()
+                across(piece, t).start()
 
         def take(order):
+            all_of(buf.at[0], send.at[0], recv.at[order]).wait_recv()
             for direction in range(2):
                 slot = tp_at[2] if order == 2 else came(direction)
-                hop(direction, order, slot).wait_recv()
                 if order == 0:
                     hop(direction, 2, slot).start()
-                index = 2 if order == 2 else (3 if direction == 0 else 1)
-                across(index, piece_of(direction, order), slot).start()
+                across(piece_of(direction, order), slot).start()
 
         def take_across():
-            for index in range(4):
-                slot = 2 * x_at[index] + (1 - core)
-                for piece in range(2):
-                    across(index, piece, slot).wait_recv()
+            all_of(buf.at[0:4], dsend.at[0], drecv.at[0]).wait_recv()
 
         def drain():
-            for direction in range(2):
-                for order in range(3):
-                    slot = came(direction) if order == 2 else t
-                    hop(direction, order, slot).wait_send()
-            for index in range(4):
-                for piece in range(2):
-                    across(index, piece, tp_at[index]).wait_send()
+            all_of(buf.at[0:3], send.at[0], recv.at[0]).wait_send()
+            all_of(buf.at[0:4], dsend.at[0], drecv.at[0]).wait_send()
 
         return start_own, take, take_across, drain
 
     wo_start, wo_take, wo_take_across, wo_drain = gather_ops(wo, wo_send, wo_recv, wo_dsend, wo_drecv)
-    nb_start, nb_take, nb_take_across, nb_drain = gather_ops(nb, nb_send, nb_recv, nb_dsend, nb_drecv)
+
+    def nb_copy(off, slot):
+        ref = nb.at[slot]
+        return remote(ref, ref, nb_send.at[0], nb_recv.at[off - 1], {"tp": tp_at[off]})
+
+    def nb_across(slot):
+        ref = nb.at[slot]
+        return remote(ref, ref, nb_dsend.at[0], nb_drecv.at[0], {"tp": sibling})
+
+    def nb_start():
+        for off in (2, 1, 3):
+            nb_copy(off, t).start()
+        nb_across(t).start()
+
+    def nb_take():
+        for off in (1, 3, 2):
+            slot = tp_at[(NX - off) % NX]
+            nb_copy(off, slot).wait_recv()
+            nb_across(slot).start()
 
     loads[6].wait()
     wo_start()
@@ -198,6 +210,7 @@
 
             @pl.when((z < NZ - 1) & ((step < HALF - 1) | (chunk < CHUNKS // 2)))
             def _():
+                up(step, chunk, low).wait_send()
                 up(step + 1, chunk, low).start()
 
         @pl.when(high < HALF)
@@ -206,6 +219,10 @@
 
             @pl.when((step < HALF - 1) | (chunk >= CHUNKS // 2))
             def _():
+                @pl.when((z + step - 1) % NZ < HALF)
+                def _():
+                    down(step, chunk, high).wait_send()
+
                 down(step + 1, chunk, high).start()
 
     with jax.named_scope("first_pass"):
@@ -213,8 +230,7 @@
             pass_on(1, chunk)
 
     with jax.named_scope("wait_q"):
-        for off in (1, 3, 2):
-            q_copy(off, y_at[(NY - off) % NY]).wait_recv()
+        all_of(qbuf.at[0 : NY - 1], q_send.at[0], q_recv.at[0]).wait_recv()
 
     def split_queries(block, _):
         q = qbuf[block].astype(F32) * scale
@@ -235,68 +251,92 @@
             jnp.concatenate((kv[slot, 2], kv[slot, 3]), axis=1),
         )
 
-    def attend(blocks, slots, own=False):
+    groups = rows // 8
+
+    def allowed(block):
+        k_pos = y * rows + lax.broadcasted_iota(jnp.int32, (rows, rows), 0)
+        q_pos = block * rows + lax.broadcasted_iota(jnp.int32, (rows, rows), 1)
+        return k_pos <= q_pos
+
+    def score(unit, keys, own=False):
+        pick, block = unit
+        found = [dot(one, qz[pick, block]) for one in keys]
+        if own:
+            found = [jnp.where(allowed(block), one, masked_score) for one in found]
+        highest = None
+        for one in found:
+            top = jnp.max(one.reshape(groups, 8, rows), axis=0)
+            highest = top if highest is None else jnp.maximum(highest, top)
+        return found, highest
+
+    def keep(ahead):
+        found, highest = ahead
+        for index, one in enumerate(found):
+            ahead_ref[index] = one
+        ahead_max[...] = highest
+
+    def absorb(unit, vals, found, highest, own=False):
+        pick, block = unit
+        now = jnp.broadcast_to(jnp.max(highest, axis=0, keepdims=True), (8, rows))
+        if not own:
+            before = m_ref[pick, block]
+            now = jnp.maximum(before, now)
+            rescale = jnp.exp2(before - now)
+        total = None
+        parts = []
+        for one in found:
+            part = jnp.exp2(one.reshape(groups, 8, rows) - now[None])
+            if own:
+                part = jnp.where(allowed(block).reshape(groups, 8, rows), part, 0.0)
+            summed = jnp.sum(part, axis=0)
+            total = summed if total is None else total + summed
+            parts.append(part.reshape(rows, rows).astype(BF16))
+        added = dot(vals, jnp.concatenate(parts, axis=0))
+        m_ref[pick, block] = now
+        if own:
+            l_ref[pick, block] = total
+            acc_ref[pick, block] = added
+        else:
+            l_ref[pick, block] = l_ref[pick, block] * rescale + total
+            kept = acc_ref[pick, block].reshape(head_v // 8, 8, rows) * rescale[None]
+            acc_ref[pick, block] = kept.reshape(head_v, rows) + added
+
+    def attend(blocks, slots, own=False, carried=False, then=None):
         keys, vals = zip(*[block_of(slot) for slot in slots])
         vals = jnp.concatenate(vals, axis=1)
         units = [(pick, block) for block in blocks for pick in range(2)]
-        groups = rows // 8
-
-        def allowed(block):
-            k_pos = y * rows + lax.broadcasted_iota(jnp.int32, (rows, rows), 0)
-            q_pos = block * rows + lax.broadcasted_iota(jnp.int32, (rows, rows), 1)
-            return k_pos <= q_pos
-
-        def score(unit):
-            pick, block = unit
-            found = [dot(one, qz[pick, block]) for one in keys]
-            if own:
-                found = [jnp.where(allowed(block), one, masked_score) for one in found]
-            highest = None
-            for one in found:
-                top = jnp.max(one.reshape(groups, 8, rows), axis=0)
-                highest = top if highest is None else jnp.maximum(highest, top)
-            return found, highest
-
-        def absorb(unit, found, highest):
-            pick, block = unit
-            now = jnp.broadcast_to(jnp.max(highest, axis=0, keepdims=True), (8, rows))
-            if not own:
-                before = m_ref[pick, block]
-                now = jnp.maximum(before, now)
-                rescale = jnp.exp2(before - now)
-            total = None
-            parts = []
-            for one in found:
-                part = jnp.exp2(one.reshape(groups, 8, rows) - now[None])
-                if own:
-                    part = jnp.where(allowed(block).reshape(groups, 8, rows), part, 0.0)
-                summed = jnp.sum(part, axis=0)
-                total = summed if total is None else total + summed
-                parts.append(part.reshape(rows, rows).astype(BF16))
-            added = dot(vals, jnp.concatenate(parts, axis=0))
-            m_ref[pick, block] = now
-            if own:
-                l_ref[pick, block] = total
-                acc_ref[pick, block] = added
-            else:
-                l_ref[pick, block] = l_ref[pick, block] * rescale + total
-                kept = acc_ref[pick, block].reshape(head_v // 8, 8, rows) * rescale[None]
-                acc_ref[pick, block] = kept.reshape(head_v, rows) + added
-
-        ahead = score(units[0])
+        if carried:
+            ahead = ([ahead_ref[index] for index in range(len(slots))], ahead_max[...])
+        else:
+            ahead = score(units[0], keys, own)
         for index, unit in enumerate(units):
             here = ahead
             if index + 1 < len(units):
-                ahead = score(units[index + 1])
-            absorb(unit, *here)
+                ahead = score(units[index + 1], keys, own)
+            elif then is not None:
+                next_block, next_slots = then
+                keep(score((0, next_block), [block_of(slot)[0] for slot in next_slots]))
+            absorb(unit, vals, *here, own)
 
     def attend_pair(step, part):
         low, high = (z + NZ - step) % NZ, (z + step) % NZ
         blocks = (2 * part, 2 * part + 1)
+        final = (step == HALF - 1) & (part == 1)
 
         @pl.when(z >= NZ - step)
         def _():
-            attend(blocks, (low, high))
+            @pl.when((z == NZ - step) & (part == 0))
+            def _():
+                keep(score((0, blocks[0]), [block_of(low)[0], block_of(high)[0]]))
+
+            @pl.when(jnp.logical_not(final))
+            def _():
+                next_slots = ((z + NZ - step - part) % NZ, (z + step + part) % NZ)
+                attend(blocks, (low, high), carried=True, then=(2 - 2 * part, next_slots))
+
+            @pl.when(final)
+            def _():
+                attend(blocks, (low, high), carried=True)
 
         @pl.when((z >= step) & (z < NZ - step))
         def _():
@@ -307,27 +347,27 @@
     def o_copy(direction, piece, slot):
         to = y_at[1] if direction == 0 else y_at[3]
         return remote(
-            opart.at[slot, piece], orecv.at[direction, piece],
-            o_send.at[direction, piece], o_recv.at[direction, piece], {"sp_1": to},
+            opart.at[slot, piece], orecv.at[piece, direction],
+            o_send.at[0], o_recv.at[piece], {"sp_1": to},
         )
 
     def rel_copy(direction, slot):
         to = y_at[1] if direction == 0 else y_at[3]
         return remote(
             opart.at[slot, direction], relay.at[direction],
-            rel_send.at[direction, 0], rel_recv.at[direction, 0], {"sp_1": to},
+            o_send.at[0], rel_recv.at[direction], {"sp_1": to},
         )
 
     def rel_forward(direction):
         to = y_at[1] if direction == 0 else y_at[3]
         return remote(
-            relay.at[direction], orecv.at[2, direction],
-            rel_send.at[direction, 1], rel_recv.at[direction, 1], {"sp_1": to},
+            relay.at[direction], orecv.at[direction, 2],
+            o_send.at[0], o_recv.at[direction], {"sp_1": to},
         )
 
     def st_copy(off, slot):
         return remote(
-            stats.at[slot], strecv.at[off], st_send.at[off], st_recv.at[off], {"sp_1": y_at[off]}
+            stats.at[slot], strecv.at[off], st_send.at[0], st_recv.at[0], {"sp_1": y_at[off]}
         )
 
     def pack(block):
@@ -375,8 +415,7 @@
             rel_forward(direction).start()
 
     def finish_combine():
-        for off in range(1, NY):
-            st_copy(off, y_at[0]).wait_recv()
+        all_of(strecv.at[1:NY], st_send.at[0], st_recv.at[0]).wait_recv()
         lam = lam_ref[0]
         tables = [stats[y], strecv[1], strecv[3], strecv[2]]
         coefs = []
@@ -394,15 +433,13 @@
             coefs.append([share * factor for share in shares])
         gain = gain_ref[...].reshape(1, head_v)
         for piece in range(2):
-            o_copy(0, piece, y_at[1]).wait_recv()
-            o_copy(1, piece, y_at[3]).wait_recv()
-            rel_forward(piece).wait_recv()
+            all_of(orecv.at[piece], o_send.at[0], o_recv.at[piece]).wait_recv()
             span = slice(piece * half_rows, (piece + 1) * half_rows)
             mixed = None
             for pick in range(2):
                 parts = [acc_ref[pick, y][:, span]]
                 for source in range(3):
-                    one = orecv[source, piece, pick * head_v : (pick + 1) * head_v]
+                    one = orecv[piece, source, pick * head_v : (pick + 1) * head_v]
                     parts.append(one.astype(F32))
                 for part, coef in zip(parts, coefs[pick]):
                     term = part * coef[:, span]
@@ -412,9 +449,7 @@
         nb_start()
 
     def finish_gather():
-        nb_take(0)
-        nb_take(1)
-        nb_take(2)
+        nb_take()
 
     loads[7].wait()
     loads[8].wait()
@@ -474,6 +509,19 @@
         with jax.named_scope("finish_relay"):
             finish_relay()
 
+    with jax.named_scope("drain_ring"):
+        for chunk in range(CHUNKS):
+
+            @pl.when(z < NZ - 1)
+            def _(chunk=chunk):
+                up(1, chunk, z).wait_send()
+
+            @pl.when((z < HALF) | (z > HALF + 1) | ((z == HALF + 1) & (chunk >= CHUNKS // 2)))
+            def _(chunk=chunk):
+                down(1, chunk, z).wait_send()
+
+        all_of(qbuf.at[0 : NY - 1], q_send.at[0], q_recv.at[0]).wait_send()
+
     with jax.named_scope("wo_far"):
         wo_take(2)
 
@@ -481,12 +529,20 @@
     def _():
         with jax.named_scope("finish_combine"):
             finish_combine()
+
+    with jax.named_scope("drain_parts"):
+        all_of(stats.at[0 : NY - 1], st_send.at[0], st_recv.at[0]).wait_send()
+        all_of(opart, o_send.at[0], o_recv.at[0]).wait_send()
+        wo_take_across()
+        wo_drain()
+
+    @pl.when(z > 0)
+    def _():
         with jax.named_scope("finish_gather"):
             finish_gather()
 
     with jax.named_scope("take_across"):
-        wo_take_across()
-        nb_take_across()
+        all_of(nb.at[0:4], nb_dsend.at[0], nb_drecv.at[0]).wait_recv()
 
     with jax.named_scope("out_proj"):
         lhs = jnp.concatenate([nb[head].reshape(rows, head_v) for head in range(2 * NX)], axis=1)
@@ -495,31 +551,9 @@
             rhs = wo[:, :, :, left : left + width].reshape(2 * NX * head_v, width)
             out_ref[:, left : left + width] = dot(lhs, rhs).astype(BF16)
 
-    def drain_ring(index, _):
-        step, chunk = index // CHUNKS, index % CHUNKS
-
-        @pl.when((z < NZ - 1) & (z + 1 >= step) & ((step < HALF) | (chunk < CHUNKS // 2)))
-        def _():
-            up(step, chunk, z).wait_send()
-
-        @pl.when(((z + step - 1) % NZ < HALF) & ((step < HALF) | (chunk >= CHUNKS // 2)))
-        def _():
-            down(step, chunk, z).wait_send()
-
-        return 0
-
     with jax.named_scope("drain"):
-        lax.fori_loop(CHUNKS, (HALF + 1) * CHUNKS, drain_ring, 0)
-        for off in range(1, NY):
-            q_copy(off, y).wait_send()
-            st_copy(off, y).wait_send()
-        for direction in range(2):
-            for piece in range(2):
-                o_copy(direction, piece, y).wait_send()
-            rel_copy(direction, y).wait_send()
-            rel_forward(direction).wait_send()
-        wo_drain()
-        nb_drain()
+        all_of(nb.at[0:3], nb_send.at[0], nb_recv.at[0]).wait_send()
+        all_of(nb.at[0:4], nb_dsend.at[0], nb_drecv.at[0]).wait_send()
 
 
 def shards(
@@ -540,36 +574,37 @@
         pltpu.VMEM((head_v,), F32),
         dma((9,)),
         pltpu.VMEM((NZ, CHUNKS, half, head_v), BF16),
-        dma((2, HALF, CHUNKS)),
+        dma((2, CHUNKS)),
         dma((2, HALF, CHUNKS)),
         pltpu.VMEM((NY, 2 * head_qk, rows), BF16),
         pltpu.VMEM((2, NY, 4 * head_qk, rows), BF16),
-        dma((NY,)),
-        dma((NY,)),
+        dma((1,)),
+        dma((1,)),
         pltpu.VMEM((2, NY, 8, rows), F32),
         pltpu.VMEM((2, NY, 8, rows), F32),
         pltpu.VMEM((2, NY, head_v, rows), F32),
+        pltpu.VMEM((2, rows, rows), F32),
+        pltpu.VMEM((8, rows), F32),
         pltpu.VMEM((NY, 2, 2 * head_v, half), BF16),
         pltpu.VMEM((NY, 8, rows), F32),
-        pltpu.VMEM((3, 2, 2 * head_v, half), BF16),
+        pltpu.VMEM((2, 3, 2 * head_v, half), BF16),
         pltpu.VMEM((NY, 8, rows), F32),
         pltpu.VMEM((2, 2 * head_v, half), BF16),
-        dma((2, 2)),
-        dma((2, 2)),
-        dma((2, 2)),
-        dma((2, 2)),
-        dma((NY,)),
-        dma((NY,)),
+        dma((1,)),
+        dma((2,)),
+        dma((2,)),
+        dma((1,)),
+        dma((1,)),
         pltpu.VMEM((heads, 2, head_v // 2, out_proj.shape[1]), BF16),
-        dma((2, 3)),
-        dma((2, 3)),
-        dma((4, 2)),
-        dma((4, 2)),
+        dma((1,)),
+        dma((3,)),
+        dma((1,)),
+        dma((1,)),
         pltpu.VMEM((heads, 2, half, head_v), BF16),
-        dma((2, 3)),
-        dma((2, 3)),
-        dma((4, 2)),
-        dma((4, 2)),
+        dma((1,)),
+        dma((3,)),
+        dma((1,)),
+        dma((1,)),
     ]
     return pl.pallas_call(
         kernel,

time: 57.2 us -> 53.5 us (0.935)
  Pallas kernels: 55.4 us -> 51.7 us
    pallas_call x1, Pallas kernels: 55.4 us -> 51.7 us  [shards(): pl.pallas_call(kernel, out_shape=pltpu.VMEM((rows, out_proj.shape[1]), BF...]
where the time goes in v4:
time: 53.5 us; the launch traced here: 53.3 us
  Pallas kernels  51.7 us (97%)
  local copies, waits for them, and re-layouts  0.97 us (2%)
  between operations  0.66 us (1%)
    pallas_call x1, Pallas kernels, shards(): pl.pallas_call(kernel, out_shape=pltpu.VMEM((rows, out_proj.shape[1]), BF...  51.7 us

profile of v4, /device:TPU:385, one launch (start us, length us, event | category | flops | bytes accessed | tf_op | source)
XLA Modules:
  0.0 53.3 jit_solution(16691299980154897893)
XLA Ops:
  0.7 51.7 %shard_map.91 = bf16[256,2048]{1,0:T(8,128)(2,1)S(1)} custom-call(bf16[256,2048]{1,0:T(8,128)(2,1)} %hidden_hbm.1, bf16[64,2048]{1,0:T(8,128)(2,1)} %bitcast.6, bf16[64,2048]{1,0:T(8,128)(2,1)} %bitcast.7, bf16[64,2048]{1,0:T(8,128)(2,1)} %bitcast.8, bf16[64,2048]{1,0:T(8,128)(2,1)} %bitcast.9, bf16[2048,128]{1,0:T(8,128)(2,1)} %wv_hbm.1, ...), custom_call_target="tpu_custom_call" | custom-call | tf_op jit(solution)/shard_map/pallas_call | solution.py:609
  52.4 1.0 %copy.11 = bf16[256,2048]{1,0:T(8,128)(2,1)} copy(bf16[256,2048]{1,0:T(8,128)(2,1)S(1)} %shard_map.91) | data formatting | bytes 2097152

commit v5 on v4

--- a/solution.py
+++ b/solution.py
@@ -31,9 +31,10 @@
     kv, kv_send, kv_recv,
     qbuf, qz, q_send, q_recv,
     m_ref, l_ref, acc_ref, ahead_ref, ahead_max,
-    opart, stats, orecv, strecv, relay, o_send, o_recv, rel_recv, st_send, st_recv,
+    opart, stats, orecv, strecv, relay, o_send, o_recv, rel_send, rel_recv, st_send, st_recv,
     wo, wo_send, wo_recv, wo_dsend, wo_drecv,
     nb, nb_send, nb_recv, nb_dsend, nb_drecv,
+    out_acc,
 ):
     z = lax.axis_index("sp_0")
     y = lax.axis_index("sp_1")
@@ -70,6 +71,7 @@
     partners = [
         {"sp_0": z_up}, {"sp_0": z_down},
         {"sp_1": y_at[1]}, {"sp_1": y_at[2]}, {"sp_1": y_at[3]},
+        {"sp_1": y_at[1], "tp": sibling}, {"sp_1": y_at[3], "tp": sibling},
         {"tp": tp_at[1]}, {"tp": tp_at[2]}, {"tp": tp_at[3]}, {"tp": sibling},
     ]
     for partner in partners:
@@ -84,21 +86,6 @@
     def dot(a, b, dims=((1,), (0,))):
         return lax.dot_general(a, b, (dims, ((), ())), preferred_element_type=F32)
 
-    with jax.named_scope("load_kv"):
-        for load in loads[:4]:
-            load.wait()
-    with jax.named_scope("proj_kv"):
-        h = hid[...]
-        k = dot(h, wk[...].reshape(2 * head_qk, wk.shape[2]), ((1,), (1,))).astype(BF16)
-        v = dot(h, wv[...]).T.astype(BF16)
-        kv[z, 0] = k[:half_rows]
-        kv[z, 1] = k[half_rows:]
-        kv[z, 2] = v[:, :half_rows]
-        kv[z, 3] = v[:, half_rows:]
-
-    with jax.named_scope("entry_barrier"):
-        pl.semaphore_wait(barrier, len(partners))
-
     def up(step, chunk, slot):
         ref = kv.at[slot, chunk]
         return remote(
@@ -111,15 +98,34 @@
             ref, ref, kv_send.at[1, chunk], kv_recv.at[1, step - 1, chunk], {"sp_0": z_down}
         )
 
-    @pl.when(z < NZ - 1)
-    def _():
-        for chunk in range(CHUNKS):
-            up(1, chunk, z).start()
-
-    @pl.when(z < HALF)
-    def _():
-        for chunk in range(CHUNKS):
-            down(1, chunk, z).start()
+    def start_ring(chunks):
+        @pl.when(z < NZ - 1)
+        def _():
+            for chunk in chunks:
+                up(1, chunk, z).start()
+
+        @pl.when(z < HALF)
+        def _():
+            for chunk in chunks:
+                down(1, chunk, z).start()
+
+    with jax.named_scope("load_kv"):
+        for load in loads[:3]:
+            load.wait()
+    with jax.named_scope("proj_k"):
+        h = hid[...]
+        k = dot(h, wk[...].reshape(2 * head_qk, wk.shape[2]), ((1,), (1,))).astype(BF16)
+        kv[z, 0] = k[:half_rows]
+        kv[z, 1] = k[half_rows:]
+    with jax.named_scope("entry_barrier"):
+        pl.semaphore_wait(barrier, len(partners))
+    start_ring((0, 1))
+    with jax.named_scope("proj_v"):
+        loads[3].wait()
+        v = dot(h, wv[...]).T.astype(BF16)
+        kv[z, 2] = v[:, :half_rows]
+        kv[z, 3] = v[:, half_rows:]
+    start_ring((2, 3))
 
     with jax.named_scope("proj_q"):
         loads[4].wait()
@@ -128,13 +134,13 @@
 
     def q_copy(off, slot):
         return remote(
-            qbuf.at[slot], qbuf.at[slot], q_send.at[0], q_recv.at[0], {"sp_1": y_at[off]}
+            qbuf.at[slot], qbuf.at[slot], q_send.at[0], q_recv.at[off - 1], {"sp_1": y_at[off]}
         )
 
     def all_of(ref, send_sem, recv_sem):
         return remote(ref, ref, send_sem, recv_sem, {"tp": sibling})
 
-    for off in (2, 1, 3):
+    for off in (3, 2, 1):
         q_copy(off, y).start()
 
     def gather_ops(buf, send, recv, dsend, drecv):
@@ -229,20 +235,23 @@
         for chunk in range(CHUNKS):
             pass_on(1, chunk)
 
-    with jax.named_scope("wait_q"):
-        all_of(qbuf.at[0 : NY - 1], q_send.at[0], q_recv.at[0]).wait_recv()
-
-    def split_queries(block, _):
+    def split_queries(block):
         q = qbuf[block].astype(F32) * scale
         high = q.astype(BF16)
         low = (q - high.astype(F32)).astype(BF16)
         nothing = jnp.zeros((head_qk, rows), BF16)
         qz[0, block] = jnp.concatenate((high[:head_qk], nothing, low[:head_qk], nothing), axis=0)
         qz[1, block] = jnp.concatenate((nothing, high[head_qk:], nothing, low[head_qk:]), axis=0)
-        return 0
-
-    with jax.named_scope("split_q"):
-        lax.fori_loop(0, NY, split_queries, 0)
+
+    def take_queries(first):
+        if first:
+            q_copy(3, y_at[1]).wait_recv()
+        else:
+            q_copy(2, y_at[2]).wait_recv()
+            q_copy(1, y_at[3]).wait_recv()
+        for off in (0, 1) if first else (2, 3):
+            split_queries(y_at[off])
+
 
     def block_of(slot):
         keys = jnp.concatenate((kv[slot, 0], kv[slot, 1]), axis=0)
@@ -320,7 +329,7 @@
 
     def attend_pair(step, part):
         low, high = (z + NZ - step) % NZ, (z + step) % NZ
-        blocks = (2 * part, 2 * part + 1)
+        blocks = ((y + 2 * part) % NY, (y + 2 * part + 1) % NY)
         final = (step == HALF - 1) & (part == 1)
 
         @pl.when(z >= NZ - step)
@@ -332,7 +341,7 @@
             @pl.when(jnp.logical_not(final))
             def _():
                 next_slots = ((z + NZ - step - part) % NZ, (z + step + part) % NZ)
-                attend(blocks, (low, high), carried=True, then=(2 - 2 * part, next_slots))
+                attend(blocks, (low, high), carried=True, then=((y + 2 - 2 * part) % NY, next_slots))
 
             @pl.when(final)
             def _():
@@ -351,18 +360,18 @@
             o_send.at[0], o_recv.at[piece], {"sp_1": to},
         )
 
-    def rel_copy(direction, slot):
+    def rel_copy(head, direction, slot):
         to = y_at[1] if direction == 0 else y_at[3]
         return remote(
-            opart.at[slot, direction], relay.at[direction],
-            o_send.at[0], rel_recv.at[direction], {"sp_1": to},
-        )
-
-    def rel_forward(direction):
+            opart.at[slot, direction], relay.at[head, direction],
+            o_send.at[0], rel_recv.at[head, direction], {"sp_1": to, "tp": 2 * x + 1},
+        )
+
+    def rel_forward(head, direction):
         to = y_at[1] if direction == 0 else y_at[3]
         return remote(
-            relay.at[direction], orecv.at[direction, 2],
-            o_send.at[0], o_recv.at[direction], {"sp_1": to},
+            relay.at[head, direction], orecv.at[direction, 2],
+            rel_send.at[head], o_recv.at[direction], {"sp_1": to, "tp": 2 * x + head},
         )
 
     def st_copy(off, slot):
@@ -390,8 +399,8 @@
                 attend((y_at[2], y_at[1]), (opposite,))
 
         pack(y_at[2])
-        rel_copy(0, y_at[2]).start()
-        rel_copy(1, y_at[2]).start()
+        rel_copy(core, 0, y_at[2]).start()
+        rel_copy(core, 1, y_at[2]).start()
         st_copy(2, y_at[2]).start()
         pack(y_at[1])
         o_copy(0, 0, y_at[1]).start()
@@ -409,10 +418,12 @@
         st_copy(3, y_at[3]).start()
         pack(y_at[0])
 
-    def finish_relay():
-        for direction in range(2):
-            rel_copy(direction, y_at[2]).wait_recv()
-            rel_forward(direction).start()
+    def finish_relay(head):
+        @pl.when(core == 1)
+        def _():
+            for direction in range(2):
+                rel_copy(head, direction, y_at[2]).wait_recv()
+                rel_forward(head, direction).start()
 
     def finish_combine():
         all_of(strecv.at[1:NY], st_send.at[0], st_recv.at[0]).wait_recv()
@@ -448,9 +459,6 @@
             nb[t, piece] = ((mixed * spread).T * gain).astype(BF16)
         nb_start()
 
-    def finish_gather():
-        nb_take()
-
     loads[7].wait()
     loads[8].wait()
 
@@ -467,9 +475,20 @@
 
         @pl.when(step == 2)
         def _():
-            attend((2 * part, 2 * part + 1), (z,), own=True)
+            @pl.when(part == 0)
+            def _():
+                with jax.named_scope("take_q"):
+                    take_queries(True)
+
+            attend(((y + 2 * part) % NY, (y + 2 * part + 1) % NY), (z,), own=True)
 
         pass_one(2 * part + 1)
+
+        @pl.when(index == 4)
+        def _():
+            with jax.named_scope("take_more_q"):
+                take_queries(False)
+
         with jax.named_scope("attend_pair"):
             attend_pair(step - 1, part)
 
@@ -481,11 +500,18 @@
         def _():
             wo_take(1)
 
-        for at, phase in ((5, lambda: finish_send(False)), (7, finish_relay), (10, finish_combine), (14, finish_gather)):
-
-            @pl.when((z == 0) & (index == at))
-            def _(phase=phase):
-                phase()
+        @pl.when(index == 16)
+        def _():
+            wo_take(2)
+
+        @pl.when((z == 0) & (index == 6))
+        def _():
+            finish_send(False)
+
+        @pl.when((z == 0) & (index == 15))
+        def _():
+            finish_relay(1)
+            finish_relay(0)
 
         return 0
 
@@ -507,7 +533,7 @@
         with jax.named_scope("finish_send"):
             finish_send(True)
         with jax.named_scope("finish_relay"):
-            finish_relay()
+            finish_relay(1)
 
     with jax.named_scope("drain_ring"):
         for chunk in range(CHUNKS):
@@ -522,34 +548,67 @@
 
         all_of(qbuf.at[0 : NY - 1], q_send.at[0], q_recv.at[0]).wait_send()
 
-    with jax.named_scope("wo_far"):
-        wo_take(2)
+    with jax.named_scope("finish_combine"):
+        finish_combine()
 
     @pl.when(z > 0)
     def _():
-        with jax.named_scope("finish_combine"):
-            finish_combine()
+        with jax.named_scope("relay_other"):
+            finish_relay(0)
 
     with jax.named_scope("drain_parts"):
         all_of(stats.at[0 : NY - 1], st_send.at[0], st_recv.at[0]).wait_send()
-        all_of(opart, o_send.at[0], o_recv.at[0]).wait_send()
+        all_of(opart.at[0:3], o_send.at[0], o_recv.at[0]).wait_send()
+
+        @pl.when(core == 1)
+        def _():
+            for head in range(2):
+                all_of(relay.at[head], rel_send.at[head], o_recv.at[0]).wait_send()
+
         wo_take_across()
         wo_drain()
 
-    @pl.when(z > 0)
-    def _():
-        with jax.named_scope("finish_gather"):
-            finish_gather()
-
-    with jax.named_scope("take_across"):
+    def heads_across():
         all_of(nb.at[0:4], nb_dsend.at[0], nb_drecv.at[0]).wait_recv()
 
-    with jax.named_scope("out_proj"):
-        lhs = jnp.concatenate([nb[head].reshape(rows, head_v) for head in range(2 * NX)], axis=1)
+    def project_out(which):
+        heads = [2 * chip + which for chip in range(NX)]
+        lhs = jnp.concatenate([nb[head].reshape(rows, head_v) for head in heads], axis=1)
         width = 256
         for left in range(0, out_ref.shape[1], width):
-            rhs = wo[:, :, :, left : left + width].reshape(2 * NX * head_v, width)
-            out_ref[:, left : left + width] = dot(lhs, rhs).astype(BF16)
+            span = slice(left, left + width)
+            rhs = jnp.concatenate([wo[head, :, :, span].reshape(head_v, width) for head in heads], axis=0)
+            found = dot(lhs, rhs)
+            if which == 1:
+                out_acc[:, span] = found
+            else:
+                out_ref[:, span] = (out_acc[:, span] + found).astype(BF16)
+
+    with jax.named_scope("gather_ones"):
+
+        @pl.when(core == 1)
+        def _():
+            nb_take()
+
+        @pl.when(core == 0)
+        def _():
+            heads_across()
+
+    with jax.named_scope("out_ones"):
+        project_out(1)
+
+    with jax.named_scope("gather_zeros"):
+
+        @pl.when(core == 0)
+        def _():
+            nb_take()
+
+        @pl.when(core == 1)
+        def _():
+            heads_across()
+
+    with jax.named_scope("out_zeros"):
+        project_out(0)
 
     with jax.named_scope("drain"):
         all_of(nb.at[0:3], nb_send.at[0], nb_recv.at[0]).wait_send()
@@ -579,7 +638,7 @@
         pltpu.VMEM((NY, 2 * head_qk, rows), BF16),
         pltpu.VMEM((2, NY, 4 * head_qk, rows), BF16),
         dma((1,)),
-        dma((1,)),
+        dma((3,)),
         pltpu.VMEM((2, NY, 8, rows), F32),
         pltpu.VMEM((2, NY, 8, rows), F32),
         pltpu.VMEM((2, NY, head_v, rows), F32),
@@ -589,10 +648,11 @@
         pltpu.VMEM((NY, 8, rows), F32),
         pltpu.VMEM((2, 3, 2 * head_v, half), BF16),
         pltpu.VMEM((NY, 8, rows), F32),
-        pltpu.VMEM((2, 2 * head_v, half), BF16),
+        pltpu.VMEM((2, 2, 2 * head_v, half), BF16),
         dma((1,)),
         dma((2,)),
         dma((2,)),
+        dma((2, 2)),
         dma((1,)),
         dma((1,)),
         pltpu.VMEM((heads, 2, head_v // 2, out_proj.shape[1]), BF16),
@@ -605,6 +665,7 @@
         dma((3,)),
         dma((1,)),
         dma((1,)),
+        pltpu.VMEM((rows, out_proj.shape[1]), F32),
     ]
     return pl.pallas_call(
         kernel,

time: 53.5 us -> 52.5 us (0.981)
  Pallas kernels: 51.7 us -> 50.8 us
    pallas_call x1, Pallas kernels: 51.7 us -> 50.8 us  [shards(): pl.pallas_call(kernel, out_shape=pltpu.VMEM((rows, out_proj.shape[1]), BF...]
where the time goes in v5:
time: 52.5 us; the launch traced here: 52.4 us
  Pallas kernels  50.8 us (97%)
  local copies, waits for them, and re-layouts  0.97 us (2%)
  between operations  0.66 us (1%)
    pallas_call x1, Pallas kernels, shards(): pl.pallas_call(kernel, out_shape=pltpu.VMEM((rows, out_proj.shape[1]), BF...  50.8 us

profile of v5, /device:TPU:385, one launch (start us, length us, event | category | flops | bytes accessed | tf_op | source)
XLA Modules:
  0.0 52.4 jit_solution(4637992523761114412)
XLA Ops:
  0.7 50.8 %shard_map.91 = bf16[256,2048]{1,0:T(8,128)(2,1)S(1)} custom-call(bf16[256,2048]{1,0:T(8,128)(2,1)} %hidden_hbm.1, bf16[64,2048]{1,0:T(8,128)(2,1)} %bitcast.6, bf16[64,2048]{1,0:T(8,128)(2,1)} %bitcast.7, bf16[64,2048]{1,0:T(8,128)(2,1)} %bitcast.8, bf16[64,2048]{1,0:T(8,128)(2,1)} %bitcast.9, bf16[2048,128]{1,0:T(8,128)(2,1)} %wv_hbm.1, ...), custom_call_target="tpu_custom_call" | custom-call | tf_op jit(solution)/shard_map/pallas_call | solution.py:670
  51.4 1.0 %copy.11 = bf16[256,2048]{1,0:T(8,128)(2,1)} copy(bf16[256,2048]{1,0:T(8,128)(2,1)S(1)} %shard_map.91) | data formatting | bytes 2097152

commit v6 on v5

--- a/solution.py
+++ b/solution.py
@@ -28,7 +28,7 @@
     hidden_hbm, wq1_hbm, wq2_hbm, wk1_hbm, wk2_hbm, wv_hbm, lam_hbm, gain_hbm, wo_hbm,
     out_ref,
     hid, wq, wk, wv, lam_ref, gain_ref, load_sem,
-    kv, kv_send, kv_recv,
+    kv, kv_send, kv_recv, give_send, give_recv,
     qbuf, qz, q_send, q_recv,
     m_ref, l_ref, acc_ref, ahead_ref, ahead_max,
     opart, stats, orecv, strecv, relay, o_send, o_recv, rel_send, rel_recv, st_send, st_recv,
@@ -64,18 +64,20 @@
         pltpu.make_async_copy(gain_hbm, gain_ref, load_sem.at[7]),
         pltpu.make_async_copy(lam_hbm, lam_ref, load_sem.at[8]),
     ]
-    for load in loads:
+    for load in loads[:3]:
         load.start()
 
     barrier = pltpu.get_barrier_semaphore()
     partners = [
-        {"sp_0": z_up}, {"sp_0": z_down},
+        {"sp_0": z_up, "tp": sibling}, {"sp_0": z_down, "tp": sibling},
         {"sp_1": y_at[1]}, {"sp_1": y_at[2]}, {"sp_1": y_at[3]},
         {"sp_1": y_at[1], "tp": sibling}, {"sp_1": y_at[3], "tp": sibling},
         {"tp": tp_at[1]}, {"tp": tp_at[2]}, {"tp": tp_at[3]}, {"tp": sibling},
     ]
     for partner in partners:
         pl.semaphore_signal(barrier, inc=1, device_id=partner, device_id_type=MESH)
+    for load in loads[3:]:
+        load.start()
 
     def remote(src, dst, send_sem, recv_sem, device):
         return pltpu.make_async_remote_copy(
@@ -86,16 +88,23 @@
     def dot(a, b, dims=((1,), (0,))):
         return lax.dot_general(a, b, (dims, ((), ())), preferred_element_type=F32)
 
+    def hop_copy(direction, step, chunk, slot, to):
+        return remote(
+            kv.at[(step - 1) % 2, slot, chunk], kv.at[step % 2, slot, chunk],
+            kv_send.at[direction, chunk], kv_recv.at[direction, step - 1, chunk],
+            {"sp_0": to, "tp": sibling},
+        )
+
     def up(step, chunk, slot):
-        ref = kv.at[slot, chunk]
+        return hop_copy(0, step, chunk, slot, z_up)
+
+    def down(step, chunk, slot):
+        return hop_copy(1, step, chunk, slot, z_down)
+
+    def give(direction, step, chunk, slot):
         return remote(
-            ref, ref, kv_send.at[0, chunk], kv_recv.at[0, step - 1, chunk], {"sp_0": z_up}
-        )
-
-    def down(step, chunk, slot):
-        ref = kv.at[slot, chunk]
-        return remote(
-            ref, ref, kv_send.at[1, chunk], kv_recv.at[1, step - 1, chunk], {"sp_0": z_down}
+            kv.at[1, slot, chunk], kv.at[0, slot, chunk],
+            give_send.at[direction, chunk], give_recv.at[direction, step // 2, chunk], {"tp": sibling},
         )
 
     def start_ring(chunks):
@@ -115,16 +124,16 @@
     with jax.named_scope("proj_k"):
         h = hid[...]
         k = dot(h, wk[...].reshape(2 * head_qk, wk.shape[2]), ((1,), (1,))).astype(BF16)
-        kv[z, 0] = k[:half_rows]
-        kv[z, 1] = k[half_rows:]
+        kv[0, z, 0] = k[:half_rows]
+        kv[0, z, 1] = k[half_rows:]
     with jax.named_scope("entry_barrier"):
         pl.semaphore_wait(barrier, len(partners))
     start_ring((0, 1))
     with jax.named_scope("proj_v"):
         loads[3].wait()
         v = dot(h, wv[...]).T.astype(BF16)
-        kv[z, 2] = v[:, :half_rows]
-        kv[z, 3] = v[:, half_rows:]
+        kv[0, z, 2] = v[:, :half_rows]
+        kv[0, z, 3] = v[:, half_rows:]
     start_ring((2, 3))
 
     with jax.named_scope("proj_q"):
@@ -219,6 +228,14 @@
                 up(step, chunk, low).wait_send()
                 up(step + 1, chunk, low).start()
 
+            @pl.when(step % 2 == 1)
+            def _():
+                @pl.when(step > 2)
+                def _():
+                    give(0, step, chunk, low).wait_send()
+
+                give(0, step, chunk, low).start()
+
         @pl.when(high < HALF)
         def _():
             down(step, chunk, high).wait_recv()
@@ -230,6 +247,26 @@
                     down(step, chunk, high).wait_send()
 
                 down(step + 1, chunk, high).start()
+
+            @pl.when((step % 2 == 1) & (z >= NZ - step))
+            def _():
+                @pl.when(z >= NZ - step + 2)
+                def _():
+                    give(1, step, chunk, high).wait_send()
+
+                give(1, step, chunk, high).start()
+
+    def take_given(step):
+        low, high = (z + NZ - step) % NZ, (z + step) % NZ
+        for chunk in range(CHUNKS):
+
+            @pl.when(z >= step)
+            def _(chunk=chunk):
+                give(0, step, chunk, low).wait_recv()
+
+            @pl.when(z >= NZ - step)
+            def _(chunk=chunk):
+                give(1, step, chunk, high).wait_recv()
 
     with jax.named_scope("first_pass"):
         for chunk in range(CHUNKS):
@@ -254,10 +291,10 @@
 
 
     def block_of(slot):
-        keys = jnp.concatenate((kv[slot, 0], kv[slot, 1]), axis=0)
+        keys = jnp.concatenate((kv[0, slot, 0], kv[0, slot, 1]), axis=0)
         return (
             jnp.concatenate((keys, keys), axis=1),
-            jnp.concatenate((kv[slot, 2], kv[slot, 3]), axis=1),
+            jnp.concatenate((kv[0, slot, 2], kv[0, slot, 3]), axis=1),
         )
 
     groups = rows // 8
@@ -330,20 +367,20 @@
     def attend_pair(step, part):
         low, high = (z + NZ - step) % NZ, (z + step) % NZ
         blocks = ((y + 2 * part) % NY, (y + 2 * part + 1) % NY)
-        final = (step == HALF - 1) & (part == 1)
+        leads = (part == 0) | ((step % 2 == 1) & (step < HALF - 1))
 
         @pl.when(z >= NZ - step)
         def _():
-            @pl.when((z == NZ - step) & (part == 0))
+            @pl.when(((z == NZ - step) | (step % 2 == 1)) & (part == 0))
             def _():
                 keep(score((0, blocks[0]), [block_of(low)[0], block_of(high)[0]]))
 
-            @pl.when(jnp.logical_not(final))
+            @pl.when(leads)
             def _():
                 next_slots = ((z + NZ - step - part) % NZ, (z + step + part) % NZ)
                 attend(blocks, (low, high), carried=True, then=((y + 2 - 2 * part) % NY, next_slots))
 
-            @pl.when(final)
+            @pl.when(jnp.logical_not(leads))
             def _():
                 attend(blocks, (low, high), carried=True)
 
@@ -489,6 +526,11 @@
             with jax.named_scope("take_more_q"):
                 take_queries(False)
 
+        @pl.when((step % 2 == 0) & (part == 0))
+        def _():
+            with jax.named_scope("take_given"):
+                take_given(step - 1)
+
         with jax.named_scope("attend_pair"):
             attend_pair(step - 1, part)
 
@@ -545,6 +587,14 @@
             @pl.when((z < HALF) | (z > HALF + 1) | ((z == HALF + 1) & (chunk >= CHUNKS // 2)))
             def _(chunk=chunk):
                 down(1, chunk, z).wait_send()
+
+            @pl.when(z >= 1)
+            def _(chunk=chunk):
+                give(0, 1, chunk, z).wait_send()
+
+            @pl.when(z >= NZ - HALF + 1)
+            def _(chunk=chunk):
+                give(1, 1, chunk, z).wait_send()
 
         all_of(qbuf.at[0 : NY - 1], q_send.at[0], q_recv.at[0]).wait_send()
 
@@ -632,9 +682,11 @@
         pltpu.SMEM((1,), F32),
         pltpu.VMEM((head_v,), F32),
         dma((9,)),
-        pltpu.VMEM((NZ, CHUNKS, half, head_v), BF16),
+        pltpu.VMEM((2, NZ, CHUNKS, half, head_v), BF16),
         dma((2, CHUNKS)),
         dma((2, HALF, CHUNKS)),
+        dma((2, CHUNKS)),
+        dma((2, HALF // 2, CHUNKS)),
         pltpu.VMEM((NY, 2 * head_qk, rows), BF16),
         pltpu.VMEM((2, NY, 4 * head_qk, rows), BF16),
         dma((1,)),

time: 52.5 us -> 56.3 us (1.072)
  Pallas kernels: 50.8 us -> 54.5 us
    pallas_call x1, Pallas kernels: 50.8 us -> 54.5 us  [shards(): pl.pallas_call(kernel, out_shape=pltpu.VMEM((rows, out_proj.shape[1]), BF...]
where the time goes in v6:
time: 56.3 us; the launch traced here: 56.2 us
  Pallas kernels  54.5 us (97%)
  local copies, waits for them, and re-layouts  0.97 us (2%)
  between operations  0.66 us (1%)
    pallas_call x1, Pallas kernels, shards(): pl.pallas_call(kernel, out_shape=pltpu.VMEM((rows, out_proj.shape[1]), BF...  54.5 us

profile of v6, /device:TPU:385, one launch (start us, length us, event | category | flops | bytes accessed | tf_op | source)
XLA Modules:
  0.0 56.2 jit_solution(1407190707176468505)
XLA Ops:
  0.7 54.5 %shard_map.91 = bf16[256,2048]{1,0:T(8,128)(2,1)S(1)} custom-call(bf16[256,2048]{1,0:T(8,128)(2,1)} %hidden_hbm.1, bf16[64,2048]{1,0:T(8,128)(2,1)} %bitcast.6, bf16[64,2048]{1,0:T(8,128)(2,1)} %bitcast.7, bf16[64,2048]{1,0:T(8,128)(2,1)} %bitcast.8, bf16[64,2048]{1,0:T(8,128)(2,1)} %bitcast.9, bf16[2048,128]{1,0:T(8,128)(2,1)} %wv_hbm.1, ...), custom_call_target="tpu_custom_call" | custom-call | tf_op jit(solution)/shard_map/pallas_call | solution.py:722
  55.2 1.0 %copy.11 = bf16[256,2048]{1,0:T(8,128)(2,1)} copy(bf16[256,2048]{1,0:T(8,128)(2,1)S(1)} %shard_map.91) | data formatting | bytes 2097152

commit v7 on v5

--- a/solution.py
+++ b/solution.py
@@ -33,7 +33,7 @@
     m_ref, l_ref, acc_ref, ahead_ref, ahead_max,
     opart, stats, orecv, strecv, relay, o_send, o_recv, rel_send, rel_recv, st_send, st_recv,
     wo, wo_send, wo_recv, wo_dsend, wo_drecv,
-    nb, nb_send, nb_recv, nb_dsend, nb_drecv,
+    nb, nb_send, nb_recv, nb_dsend, nb_drecv, far_send, far_recv,
     out_acc,
 ):
     z = lax.axis_index("sp_0")
@@ -64,7 +64,7 @@
         pltpu.make_async_copy(gain_hbm, gain_ref, load_sem.at[7]),
         pltpu.make_async_copy(lam_hbm, lam_ref, load_sem.at[8]),
     ]
-    for load in loads:
+    for load in loads[:3]:
         load.start()
 
     barrier = pltpu.get_barrier_semaphore()
@@ -76,6 +76,8 @@
     ]
     for partner in partners:
         pl.semaphore_signal(barrier, inc=1, device_id=partner, device_id_type=MESH)
+    for load in loads[3:]:
+        load.start()
 
     def remote(src, dst, send_sem, recv_sem, device):
         return pltpu.make_async_remote_copy(
@@ -189,20 +191,29 @@
         ref = nb.at[slot]
         return remote(ref, ref, nb_send.at[0], nb_recv.at[off - 1], {"tp": tp_at[off]})
 
-    def nb_across(slot):
+    def nb_across(kind, slot):
         ref = nb.at[slot]
-        return remote(ref, ref, nb_dsend.at[0], nb_drecv.at[0], {"tp": sibling})
+        return remote(ref, ref, nb_dsend.at[0], nb_drecv.at[kind], {"tp": sibling})
+
+    def nb_far(slot):
+        ref = nb.at[slot]
+        return remote(ref, ref, far_send.at[0], far_recv.at[0], {"tp": 2 * x_at[2] + 1})
 
     def nb_start():
-        for off in (2, 1, 3):
+        nb_across(0, t).start()
+
+        @pl.when(core == 1)
+        def _():
+            nb_copy(2, t).start()
+
+        for off in (1, 3):
             nb_copy(off, t).start()
-        nb_across(t).start()
-
-    def nb_take():
-        for off in (1, 3, 2):
+
+    def nb_take(offs):
+        for off in offs:
             slot = tp_at[(NX - off) % NX]
             nb_copy(off, slot).wait_recv()
-            nb_across(slot).start()
+            nb_across(1, slot).start()
 
     loads[6].wait()
     wo_start()
@@ -392,30 +403,28 @@
         stats[block] = jnp.concatenate(table, axis=0)
 
     def finish_send(late):
-        if late:
-
-            @pl.when(z >= HALF)
-            def _():
-                attend((y_at[2], y_at[1]), (opposite,))
-
+        def absorb_last(blocks):
+            if late:
+
+                @pl.when(z >= HALF)
+                def _():
+                    attend(blocks, (opposite,))
+
+        absorb_last((y_at[2],))
         pack(y_at[2])
         rel_copy(core, 0, y_at[2]).start()
         rel_copy(core, 1, y_at[2]).start()
         st_copy(2, y_at[2]).start()
+        absorb_last((y_at[1], y_at[3]))
         pack(y_at[1])
         o_copy(0, 0, y_at[1]).start()
         o_copy(0, 1, y_at[1]).start()
         st_copy(1, y_at[1]).start()
-        if late:
-
-            @pl.when(z >= HALF)
-            def _():
-                attend((y_at[3], y_at[0]), (opposite,))
-
         pack(y_at[3])
         o_copy(1, 0, y_at[3]).start()
         o_copy(1, 1, y_at[3]).start()
         st_copy(3, y_at[3]).start()
+        absorb_last((y_at[0],))
         pack(y_at[0])
 
     def finish_relay(head):
@@ -568,51 +577,62 @@
         wo_take_across()
         wo_drain()
 
-    def heads_across():
-        all_of(nb.at[0:4], nb_dsend.at[0], nb_drecv.at[0]).wait_recv()
-
-    def project_out(which):
-        heads = [2 * chip + which for chip in range(NX)]
+    def project_out(heads, first=False, last=False):
         lhs = jnp.concatenate([nb[head].reshape(rows, head_v) for head in heads], axis=1)
         width = 256
         for left in range(0, out_ref.shape[1], width):
             span = slice(left, left + width)
             rhs = jnp.concatenate([wo[head, :, :, span].reshape(head_v, width) for head in heads], axis=0)
             found = dot(lhs, rhs)
-            if which == 1:
+            if not first:
+                found = out_acc[:, span] + found
+            if last:
+                out_ref[:, span] = found.astype(BF16)
+            else:
                 out_acc[:, span] = found
-            else:
-                out_ref[:, span] = (out_acc[:, span] + found).astype(BF16)
 
     with jax.named_scope("gather_ones"):
 
         @pl.when(core == 1)
         def _():
-            nb_take()
+            nb_take((1, 3, 2))
 
         @pl.when(core == 0)
         def _():
-            heads_across()
+            nb_across(0, 2 * x + 1).wait_recv()
+            all_of(nb.at[0:3], nb_dsend.at[0], nb_drecv.at[1]).wait_recv()
 
     with jax.named_scope("out_ones"):
-        project_out(1)
-
-    with jax.named_scope("gather_zeros"):
-
-        @pl.when(core == 0)
-        def _():
-            nb_take()
-
-        @pl.when(core == 1)
-        def _():
-            heads_across()
-
-    with jax.named_scope("out_zeros"):
-        project_out(0)
-
-    with jax.named_scope("drain"):
+        project_out([1, 3, 5, 7], first=True)
+
+    @pl.when(core == 1)
+    def _():
+        with jax.named_scope("far_start"):
+            nb_across(0, 2 * x).wait_recv()
+            nb_far(2 * x).start()
+        with jax.named_scope("far_wait"):
+            nb_far(2 * x_at[2]).wait_recv()
+            nb_across(2, 2 * x_at[2]).start()
+        with jax.named_scope("zeros_wait"):
+            all_of(nb.at[0:2], nb_dsend.at[0], nb_drecv.at[1]).wait_recv()
+        with jax.named_scope("out_zeros"):
+            project_out([0, 2, 4, 6], last=True)
         all_of(nb.at[0:3], nb_send.at[0], nb_recv.at[0]).wait_send()
-        all_of(nb.at[0:4], nb_dsend.at[0], nb_drecv.at[0]).wait_send()
+        all_of(nb.at[0:5], nb_dsend.at[0], nb_drecv.at[0]).wait_send()
+        nb_far(2 * x).wait_send()
+
+    @pl.when(core == 0)
+    def _():
+        with jax.named_scope("near_wait"):
+            nb_take((1, 3))
+        with jax.named_scope("out_near"):
+            project_out([2 * x_at[0], 2 * x_at[1], 2 * x_at[3]])
+        with jax.named_scope("far_wait0"):
+            nb_across(2, 2 * x_at[2]).wait_recv()
+        with jax.named_scope("out_far"):
+            project_out([2 * x_at[2]], last=True)
+        all_of(nb.at[0:2], nb_send.at[0], nb_recv.at[0]).wait_send()
+        all_of(nb.at[0:3], nb_dsend.at[0], nb_drecv.at[0]).wait_send()
 
 
 def shards(
@@ -664,6 +684,8 @@
         dma((1,)),
         dma((3,)),
         dma((1,)),
+        dma((3,)),
+        dma((1,)),
         dma((1,)),
         pltpu.VMEM((rows, out_proj.shape[1]), F32),
     ]

time: 52.5 us -> 51.6 us (0.983)
  Pallas kernels: 50.8 us -> 49.8 us
    pallas_call x1, Pallas kernels: 50.8 us -> 49.8 us  [shards(): pl.pallas_call(kernel, out_shape=pltpu.VMEM((rows, out_proj.shape[1]), BF...]
where the time goes in v7:
time: 51.6 us; the launch traced here: 51.4 us
  Pallas kernels  49.8 us (97%)
  local copies, waits for them, and re-layouts  0.97 us (2%)
  between operations  0.66 us (1%)
    pallas_call x1, Pallas kernels, shards(): pl.pallas_call(kernel, out_shape=pltpu.VMEM((rows, out_proj.shape[1]), BF...  49.8 us

profile of v7, /device:TPU:385, one launch (start us, length us, event | category | flops | bytes accessed | tf_op | source)
XLA Modules:
  0.0 51.4 jit_solution(11560833520452430185)
XLA Ops:
  0.7 49.8 %shard_map.91 = bf16[256,2048]{1,0:T(8,128)(2,1)S(1)} custom-call(bf16[256,2048]{1,0:T(8,128)(2,1)} %hidden_hbm.1, bf16[64,2048]{1,0:T(8,128)(2,1)} %bitcast.6, bf16[64,2048]{1,0:T(8,128)(2,1)} %bitcast.7, bf16[64,2048]{1,0:T(8,128)(2,1)} %bitcast.8, bf16[64,2048]{1,0:T(8,128)(2,1)} %bitcast.9, bf16[2048,128]{1,0:T(8,128)(2,1)} %wv_hbm.1, ...), custom_call_target="tpu_custom_call" | custom-call | tf_op jit(solution)/shard_map/pallas_call | solution.py:692
  50.5 1.0 %copy.11 = bf16[256,2048]{1,0:T(8,128)(2,1)} copy(bf16[256,2048]{1,0:T(8,128)(2,1)S(1)} %shard_map.91) | data formatting | bytes 2097152

commit v8 on v7

--- a/solution.py
+++ b/solution.py
@@ -28,7 +28,7 @@
     hidden_hbm, wq1_hbm, wq2_hbm, wk1_hbm, wk2_hbm, wv_hbm, lam_hbm, gain_hbm, wo_hbm,
     out_ref,
     hid, wq, wk, wv, lam_ref, gain_ref, load_sem,
-    kv, kv_send, kv_recv,
+    kv, kv_send, kv_recv, skip_send,
     qbuf, qz, q_send, q_recv,
     m_ref, l_ref, acc_ref, ahead_ref, ahead_max,
     opart, stats, orecv, strecv, relay, o_send, o_recv, rel_send, rel_recv, st_send, st_recv,
@@ -69,7 +69,7 @@
 
     barrier = pltpu.get_barrier_semaphore()
     partners = [
-        {"sp_0": z_up}, {"sp_0": z_down},
+        {"sp_0": z_up}, {"sp_0": z_down}, {"sp_0": (z + 2) % NZ}, {"sp_0": (z + NZ - 2) % NZ},
         {"sp_1": y_at[1]}, {"sp_1": y_at[2]}, {"sp_1": y_at[3]},
         {"sp_1": y_at[1], "tp": sibling}, {"sp_1": y_at[3], "tp": sibling},
         {"tp": tp_at[1]}, {"tp": tp_at[2]}, {"tp": tp_at[3]}, {"tp": sibling},
@@ -100,7 +100,24 @@
             ref, ref, kv_send.at[1, chunk], kv_recv.at[1, step - 1, chunk], {"sp_0": z_down}
         )
 
+    def skip(direction, chunk):
+        ref = kv.at[z, chunk]
+        to = (z + 2) % NZ if direction == 0 else (z + NZ - 2) % NZ
+        return remote(
+            ref, ref, skip_send.at[direction], kv_recv.at[direction, 1, chunk], {"sp_0": to}
+        )
+
     def start_ring(chunks):
+        @pl.when((core == 0) & (z < NZ - 2))
+        def _():
+            for chunk in chunks:
+                skip(0, chunk).start()
+
+        @pl.when((core == 0) & (z < HALF))
+        def _():
+            for chunk in chunks:
+                skip(1, chunk).start()
+
         @pl.when(z < NZ - 1)
         def _():
             for chunk in chunks:
@@ -220,12 +237,13 @@
 
     def pass_on(step, chunk):
         low, high = (z + NZ - step) % NZ, (z + step) % NZ
+        onward = (core == 1) | (step > 1)
 
         @pl.when(z >= step)
         def _():
             up(step, chunk, low).wait_recv()
 
-            @pl.when((z < NZ - 1) & ((step < HALF - 1) | (chunk < CHUNKS // 2)))
+            @pl.when(onward & (z < NZ - 1) & ((step < HALF - 1) | (chunk < CHUNKS // 2)))
             def _():
                 up(step, chunk, low).wait_send()
                 up(step + 1, chunk, low).start()
@@ -234,9 +252,11 @@
         def _():
             down(step, chunk, high).wait_recv()
 
-            @pl.when((step < HALF - 1) | (chunk >= CHUNKS // 2))
+            @pl.when(onward & ((step < HALF - 1) | (chunk >= CHUNKS // 2)))
             def _():
-                @pl.when((z + step - 1) % NZ < HALF)
+                sent = ((z + step - 1) % NZ < HALF) & ((core == 1) | (step > 2))
+
+                @pl.when((z < HALF) | sent)
                 def _():
                     down(step, chunk, high).wait_send()
 
@@ -382,7 +402,7 @@
         to = y_at[1] if direction == 0 else y_at[3]
         return remote(
             relay.at[head, direction], orecv.at[direction, 2],
-            rel_send.at[head], o_recv.at[direction], {"sp_1": to, "tp": 2 * x + head},
+            rel_send.at[head], o_recv.at[2 + direction], {"sp_1": to, "tp": 2 * x + head},
         )
 
     def st_copy(off, slot):
@@ -452,18 +472,25 @@
             factor = (1.0 if pick == 0 else -lam) / total
             coefs.append([share * factor for share in shares])
         gain = gain_ref[...].reshape(1, head_v)
-        for piece in range(2):
-            all_of(orecv.at[piece], o_send.at[0], o_recv.at[piece]).wait_recv()
-            span = slice(piece * half_rows, (piece + 1) * half_rows)
-            mixed = None
-            for pick in range(2):
-                parts = [acc_ref[pick, y][:, span]]
-                for source in range(3):
-                    one = orecv[piece, source, pick * head_v : (pick + 1) * head_v]
-                    parts.append(one.astype(F32))
-                for part, coef in zip(parts, coefs[pick]):
-                    term = part * coef[:, span]
-                    mixed = term if mixed is None else mixed + term
+        spans = [slice(piece * half_rows, (piece + 1) * half_rows) for piece in range(2)]
+
+        def shares_of(part_of, index, span):
+            terms = [part_of(pick).astype(F32) * coefs[pick][index][:, span] for pick in range(2)]
+            return terms[0] + terms[1]
+
+        def arrived(piece, source):
+            return lambda pick: orecv[piece, source, pick * head_v : (pick + 1) * head_v]
+
+        near = []
+        for piece, span in enumerate(spans):
+            all_of(orecv.at[piece, 0:2], o_send.at[0], o_recv.at[piece]).wait_recv()
+            mixed = shares_of(lambda pick, span=span: acc_ref[pick, y][:, span], 0, span)
+            for source in range(2):
+                mixed = mixed + shares_of(arrived(piece, source), 1 + source, span)
+            near.append(mixed)
+        for piece, span in enumerate(spans):
+            all_of(orecv.at[piece, 2], o_send.at[0], o_recv.at[2 + piece]).wait_recv()
+            mixed = near[piece] + shares_of(arrived(piece, 2), 3, span)
             spread = lax.rsqrt(jnp.mean(mixed * mixed, axis=0, keepdims=True) + epsilon)
             nb[t, piece] = ((mixed * spread).T * gain).astype(BF16)
         nb_start()
@@ -554,6 +581,14 @@
             @pl.when((z < HALF) | (z > HALF + 1) | ((z == HALF + 1) & (chunk >= CHUNKS // 2)))
             def _(chunk=chunk):
                 down(1, chunk, z).wait_send()
+
+        @pl.when((core == 0) & (z < NZ - 2))
+        def _():
+            all_of(kv.at[0], skip_send.at[0], kv_recv.at[0, 1, 0]).wait_send()
+
+        @pl.when((core == 0) & (z < HALF))
+        def _():
+            all_of(kv.at[0], skip_send.at[1], kv_recv.at[1, 1, 0]).wait_send()
 
         all_of(qbuf.at[0 : NY - 1], q_send.at[0], q_recv.at[0]).wait_send()
 
@@ -655,6 +690,7 @@
         pltpu.VMEM((NZ, CHUNKS, half, head_v), BF16),
         dma((2, CHUNKS)),
         dma((2, HALF, CHUNKS)),
+        dma((2,)),
         pltpu.VMEM((NY, 2 * head_qk, rows), BF16),
         pltpu.VMEM((2, NY, 4 * head_qk, rows), BF16),
         dma((1,)),
@@ -670,7 +706,7 @@
         pltpu.VMEM((NY, 8, rows), F32),
         pltpu.VMEM((2, 2, 2 * head_v, half), BF16),
         dma((1,)),
-        dma((2,)),
+        dma((4,)),
         dma((2,)),
         dma((2, 2)),
         dma((1,)),

time: 51.6 us -> 54.4 us (1.054)
  Pallas kernels: 49.8 us -> 52.7 us
    pallas_call x1, Pallas kernels: 49.8 us -> 52.7 us  [shards(): pl.pallas_call(kernel, out_shape=pltpu.VMEM((rows, out_proj.shape[1]), BF...]
where the time goes in v8:
time: 54.4 us; the launch traced here: 54.3 us
  Pallas kernels  52.7 us (97%)
  local copies, waits for them, and re-layouts  0.97 us (2%)
  between operations  0.66 us (1%)
    pallas_call x1, Pallas kernels, shards(): pl.pallas_call(kernel, out_shape=pltpu.VMEM((rows, out_proj.shape[1]), BF...  52.7 us

profile of v8, /device:TPU:385, one launch (start us, length us, event | category | flops | bytes accessed | tf_op | source)
XLA Modules:
  0.0 54.3 jit_solution(16704426741944189243)
XLA Ops:
  0.7 52.7 %shard_map.91 = bf16[256,2048]{1,0:T(8,128)(2,1)S(1)} custom-call(bf16[256,2048]{1,0:T(8,128)(2,1)} %hidden_hbm.1, bf16[64,2048]{1,0:T(8,128)(2,1)} %bitcast.6, bf16[64,2048]{1,0:T(8,128)(2,1)} %bitcast.7, bf16[64,2048]{1,0:T(8,128)(2,1)} %bitcast.8, bf16[64,2048]{1,0:T(8,128)(2,1)} %bitcast.9, bf16[2048,128]{1,0:T(8,128)(2,1)} %wv_hbm.1, ...), custom_call_target="tpu_custom_call" | custom-call | tf_op jit(solution)/shard_map/pallas_call | solution.py:728
  53.3 1.0 %copy.11 = bf16[256,2048]{1,0:T(8,128)(2,1)} copy(bf16[256,2048]{1,0:T(8,128)(2,1)S(1)} %shard_map.91) | data formatting | bytes 2097152

commit v9 on v7

--- a/solution.py
+++ b/solution.py
@@ -31,7 +31,7 @@
     kv, kv_send, kv_recv,
     qbuf, qz, q_send, q_recv,
     m_ref, l_ref, acc_ref, ahead_ref, ahead_max,
-    opart, stats, orecv, strecv, relay, o_send, o_recv, rel_send, rel_recv, st_send, st_recv,
+    opart, stats, orecv, strecv, o_send, o_recv, st_send, st_recv,
     wo, wo_send, wo_recv, wo_dsend, wo_drecv,
     nb, nb_send, nb_recv, nb_dsend, nb_drecv, far_send, far_recv,
     out_acc,
@@ -71,7 +71,6 @@
     partners = [
         {"sp_0": z_up}, {"sp_0": z_down},
         {"sp_1": y_at[1]}, {"sp_1": y_at[2]}, {"sp_1": y_at[3]},
-        {"sp_1": y_at[1], "tp": sibling}, {"sp_1": y_at[3], "tp": sibling},
         {"tp": tp_at[1]}, {"tp": tp_at[2]}, {"tp": tp_at[3]}, {"tp": sibling},
     ]
     for partner in partners:
@@ -371,18 +370,10 @@
             o_send.at[0], o_recv.at[piece], {"sp_1": to},
         )
 
-    def rel_copy(head, direction, slot):
-        to = y_at[1] if direction == 0 else y_at[3]
+    def far_copy(piece, slot):
         return remote(
-            opart.at[slot, direction], relay.at[head, direction],
-            o_send.at[0], rel_recv.at[head, direction], {"sp_1": to, "tp": 2 * x + 1},
-        )
-
-    def rel_forward(head, direction):
-        to = y_at[1] if direction == 0 else y_at[3]
-        return remote(
-            relay.at[head, direction], orecv.at[direction, 2],
-            rel_send.at[head], o_recv.at[direction], {"sp_1": to, "tp": 2 * x + head},
+            opart.at[slot, piece], orecv.at[piece, 2],
+            o_send.at[0], o_recv.at[2 + piece], {"sp_1": y_at[2]},
         )
 
     def st_copy(off, slot):
@@ -412,8 +403,8 @@
 
         absorb_last((y_at[2],))
         pack(y_at[2])
-        rel_copy(core, 0, y_at[2]).start()
-        rel_copy(core, 1, y_at[2]).start()
+        far_copy(0, y_at[2]).start()
+        far_copy(1, y_at[2]).start()
         st_copy(2, y_at[2]).start()
         absorb_last((y_at[1], y_at[3]))
         pack(y_at[1])
@@ -426,13 +417,6 @@
         st_copy(3, y_at[3]).start()
         absorb_last((y_at[0],))
         pack(y_at[0])
-
-    def finish_relay(head):
-        @pl.when(core == 1)
-        def _():
-            for direction in range(2):
-                rel_copy(head, direction, y_at[2]).wait_recv()
-                rel_forward(head, direction).start()
 
     def finish_combine():
         all_of(strecv.at[1:NY], st_send.at[0], st_recv.at[0]).wait_recv()
@@ -452,18 +436,25 @@
             factor = (1.0 if pick == 0 else -lam) / total
             coefs.append([share * factor for share in shares])
         gain = gain_ref[...].reshape(1, head_v)
-        for piece in range(2):
-            all_of(orecv.at[piece], o_send.at[0], o_recv.at[piece]).wait_recv()
-            span = slice(piece * half_rows, (piece + 1) * half_rows)
-            mixed = None
-            for pick in range(2):
-                parts = [acc_ref[pick, y][:, span]]
-                for source in range(3):
-                    one = orecv[piece, source, pick * head_v : (pick + 1) * head_v]
-                    parts.append(one.astype(F32))
-                for part, coef in zip(parts, coefs[pick]):
-                    term = part * coef[:, span]
-                    mixed = term if mixed is None else mixed + term
+        spans = [slice(piece * half_rows, (piece + 1) * half_rows) for piece in range(2)]
+
+        def shares_of(part_of, index, span):
+            terms = [part_of(pick).astype(F32) * coefs[pick][index][:, span] for pick in range(2)]
+            return terms[0] + terms[1]
+
+        def arrived(piece, source):
+            return lambda pick: orecv[piece, source, pick * head_v : (pick + 1) * head_v]
+
+        near = []
+        for piece, span in enumerate(spans):
+            all_of(orecv.at[piece, 0:2], o_send.at[0], o_recv.at[piece]).wait_recv()
+            mixed = shares_of(lambda pick, span=span: acc_ref[pick, y][:, span], 0, span)
+            for source in range(2):
+                mixed = mixed + shares_of(arrived(piece, source), 1 + source, span)
+            near.append(mixed)
+        for piece, span in enumerate(spans):
+            all_of(orecv.at[piece, 2], o_send.at[0], o_recv.at[2 + piece]).wait_recv()
+            mixed = near[piece] + shares_of(arrived(piece, 2), 3, span)
             spread = lax.rsqrt(jnp.mean(mixed * mixed, axis=0, keepdims=True) + epsilon)
             nb[t, piece] = ((mixed * spread).T * gain).astype(BF16)
         nb_start()
@@ -517,11 +508,6 @@
         def _():
             finish_send(False)
 
-        @pl.when((z == 0) & (index == 15))
-        def _():
-            finish_relay(1)
-            finish_relay(0)
-
         return 0
 
     with jax.named_scope("ring"):
@@ -541,8 +527,6 @@
     def _():
         with jax.named_scope("finish_send"):
             finish_send(True)
-        with jax.named_scope("finish_relay"):
-            finish_relay(1)
 
     with jax.named_scope("drain_ring"):
         for chunk in range(CHUNKS):
@@ -560,19 +544,9 @@
     with jax.named_scope("finish_combine"):
         finish_combine()
 
-    @pl.when(z > 0)
-    def _():
-        with jax.named_scope("relay_other"):
-            finish_relay(0)
-
     with jax.named_scope("drain_parts"):
         all_of(stats.at[0 : NY - 1], st_send.at[0], st_recv.at[0]).wait_send()
         all_of(opart.at[0:3], o_send.at[0], o_recv.at[0]).wait_send()
-
-        @pl.when(core == 1)
-        def _():
-            for head in range(2):
-                all_of(relay.at[head], rel_send.at[head], o_recv.at[0]).wait_send()
 
         wo_take_across()
         wo_drain()
@@ -668,11 +642,8 @@
         pltpu.VMEM((NY, 8, rows), F32),
         pltpu.VMEM((2, 3, 2 * head_v, half), BF16),
         pltpu.VMEM((NY, 8, rows), F32),
-        pltpu.VMEM((2, 2, 2 * head_v, half), BF16),
-        dma((1,)),
-        dma((2,)),
-        dma((2,)),
-        dma((2, 2)),
+        dma((1,)),
+        dma((4,)),
         dma((1,)),
         dma((1,)),
         pltpu.VMEM((heads, 2, head_v // 2, out_proj.shape[1]), BF16),

time: 51.6 us -> 51.1 us (level)
    pallas_call x1, Pallas kernels: 49.8 us -> 49.3 us  [shards(): pl.pallas_call(kernel, out_shape=pltpu.VMEM((rows, out_proj.shape[1]), BF...]
where the time goes in v9:
time: 51.1 us; the launch traced here: 50.9 us
  Pallas kernels  49.3 us (96%)
  local copies, waits for them, and re-layouts  0.97 us (2%)
  between operations  0.66 us (1%)
    pallas_call x1, Pallas kernels, shards(): pl.pallas_call(kernel, out_shape=pltpu.VMEM((rows, out_proj.shape[1]), BF...  49.3 us

profile of v9, /device:TPU:385, one launch (start us, length us, event | category | flops | bytes accessed | tf_op | source)
XLA Modules:
  0.0 50.9 jit_solution(11826762485441130422)
XLA Ops:
  0.7 49.3 %shard_map.91 = bf16[256,2048]{1,0:T(8,128)(2,1)S(1)} custom-call(bf16[256,2048]{1,0:T(8,128)(2,1)} %hidden_hbm.1, bf16[64,2048]{1,0:T(8,128)(2,1)} %bitcast.6, bf16[64,2048]{1,0:T(8,128)(2,1)} %bitcast.7, bf16[64,2048]{1,0:T(8,128)(2,1)} %bitcast.8, bf16[64,2048]{1,0:T(8,128)(2,1)} %bitcast.9, bf16[2048,128]{1,0:T(8,128)(2,1)} %wv_hbm.1, ...), custom_call_target="tpu_custom_call" | custom-call | tf_op jit(solution)/shard_map/pallas_call | solution.py:663
  49.9 1.0 %copy.11 = bf16[256,2048]{1,0:T(8,128)(2,1)} copy(bf16[256,2048]{1,0:T(8,128)(2,1)S(1)} %shard_map.91) | data formatting | bytes 2097152

commit v10 on v9

--- a/solution.py
+++ b/solution.py
@@ -587,10 +587,12 @@
         with jax.named_scope("far_wait"):
             nb_far(2 * x_at[2]).wait_recv()
             nb_across(2, 2 * x_at[2]).start()
+        with jax.named_scope("out_far1"):
+            project_out([2 * x_at[0], 2 * x_at[2]])
         with jax.named_scope("zeros_wait"):
             all_of(nb.at[0:2], nb_dsend.at[0], nb_drecv.at[1]).wait_recv()
         with jax.named_scope("out_zeros"):
-            project_out([0, 2, 4, 6], last=True)
+            project_out([2 * x_at[1], 2 * x_at[3]], last=True)
         all_of(nb.at[0:3], nb_send.at[0], nb_recv.at[0]).wait_send()
         all_of(nb.at[0:5], nb_dsend.at[0], nb_drecv.at[0]).wait_send()
         nb_far(2 * x).wait_send()

time: 51.1 us -> 51.1 us (level)
  no operation moved by 1% of the time
where the time goes in v10:
time: 51.1 us; the launch traced here: 50.9 us
  Pallas kernels  49.3 us (96%)
  local copies, waits for them, and re-layouts  0.97 us (2%)
  between operations  0.66 us (1%)
    pallas_call x1, Pallas kernels, shards(): pl.pallas_call(kernel, out_shape=pltpu.VMEM((rows, out_proj.shape[1]), BF...  49.3 us

profile of v10, /device:TPU:385, one launch (start us, length us, event | category | flops | bytes accessed | tf_op | source)
XLA Modules:
  0.0 50.9 jit_solution(8323226649042083515)
XLA Ops:
  0.7 49.3 %shard_map.91 = bf16[256,2048]{1,0:T(8,128)(2,1)S(1)} custom-call(bf16[256,2048]{1,0:T(8,128)(2,1)} %hidden_hbm.1, bf16[64,2048]{1,0:T(8,128)(2,1)} %bitcast.6, bf16[64,2048]{1,0:T(8,128)(2,1)} %bitcast.7, bf16[64,2048]{1,0:T(8,128)(2,1)} %bitcast.8, bf16[64,2048]{1,0:T(8,128)(2,1)} %bitcast.9, bf16[2048,128]{1,0:T(8,128)(2,1)} %wv_hbm.1, ...), custom_call_target="tpu_custom_call" | custom-call | tf_op jit(solution)/shard_map/pallas_call | solution.py:665
  50.0 1.0 %copy.11 = bf16[256,2048]{1,0:T(8,128)(2,1)} copy(bf16[256,2048]{1,0:T(8,128)(2,1)S(1)} %shard_map.91) | data formatting | bytes 2097152
